TPU v7x, 128 devices: a whole 4x4x4 slice. The times are simulated.
128 devices in a mesh: sp: 32 (over z, y, core), tp: 4 (over x).
Axes of the slice: x: 4, y: 4, z: 4, core: 2. Of those that a mesh axis runs over, the one named last changes fastest.
Arguments:
- conv_input: bfloat16 [16384, 1024], P('sp', 'tp'), may hold values from -6 to 6
- gate_inner: bfloat16 [16384, 1024], P('sp', 'tp'), may hold values from -6 to 6
- gate_outer: bfloat16 [16384, 1024], P('sp', 'tp'), may hold values from -6 to 6
- conv_taps: bfloat16 [3, 1024], P(None, 'tp'), may hold values from -3.5 to 3.5
- doc_ids: int32 [16384], P('sp'), may hold values from 0 to 15, never falling along the last dimension, each value on 1 to 2048 neighbouring positions
- residual_in: bfloat16 [16384, 2048], P(('sp', 'tp')), may hold values from -6 to 6
- out_proj: bfloat16 [1024, 2048], replicated, may hold values from -0.1875 to 0.1875
- norm_gain: float32 [2048], replicated, may hold values from 0.1 to 1.9
- expert_ids: int32 [16384, 2], P(('sp', 'tp')), may hold values from 0 to 127, all different within a row; in each aligned block of 128 rows (0 to 127, 128 to 255, ...) at most 4 rows name the same one
- expert_weights: float32 [16384, 2], P(('sp', 'tp')), may hold values from 0.2 to 1
- gate_proj: bfloat16 [128, 2048, 1024], P(('sp', 'tp')), may hold values from -0.125 to 0.125
- up_proj: bfloat16 [128, 2048, 1024], P(('sp', 'tp')), may hold values from -0.125 to 0.125
- down_proj: bfloat16 [128, 1024, 2048], P(('sp', 'tp')), may hold values from -0.1875 to 0.1875
Outputs:
- layer_out: bfloat16 [16384, 2048], P(('sp', 'tp'))
Inputs may be any that keep to these rules, and one draw needn't show every extreme that they name: `doc_ids`: never falls along positions; each document has at most 2048 positions. `expert_ids`: each row names 2 different experts; within the rows of one device, aligned blocks of 128 rows, no expert is named more than 4 times, a bound that some block reaches.
All inputs are finite; a program needn't handle non-finite values.
Results may differ from a plain program's by a relative error of at most 0.009.
Values may be sent and summed in bfloat16 or wider, within the bound.
No kernel may reach another device: no remote copies, remote signals or barrier semaphores. Data moves between devices by JAX's collectives and lax.ppermute only.
A program may use at most 64 MiB of HBM per device.

v0:
```python
import jax
import jax.numpy as jnp
from jax import lax
from jax.sharding import PartitionSpec as P


def from_behind(block, axis, distance):
    devices = range(lax.axis_size(axis))
    route = [(i - distance, i) for i in devices if i - distance in devices]
    return lax.ppermute(block, axis, route)


def expert_rows(arrived, gate_weight, up_weight, down_weight):
    gate_value = jnp.dot(arrived, gate_weight, preferred_element_type=jnp.float32)
    up_value = jnp.dot(arrived, up_weight, preferred_element_type=jnp.float32)
    hidden = (jax.nn.silu(gate_value) * up_value).astype(jnp.bfloat16)
    return jnp.dot(hidden, down_weight, preferred_element_type=jnp.float32).astype(jnp.bfloat16)


def on_device(
    conv_input,
    gate_inner,
    gate_outer,
    conv_taps,
    doc_ids,
    residual_in,
    out_proj,
    norm_gain,
    expert_ids,
    expert_weights,
    gate_proj,
    up_proj,
    down_proj,
):
    inner_prod = conv_input.astype(jnp.float32) * gate_inner.astype(jnp.float32)
    earlier, earlier_docs = from_behind((inner_prod[-2:], doc_ids[-2:]), "sp", 1)
    padded = jnp.concatenate([earlier, inner_prod], axis=0)
    padded_docs = jnp.concatenate([earlier_docs, doc_ids], axis=0)
    length = inner_prod.shape[0]
    tap_values = conv_taps.astype(jnp.float32)
    one_back = jnp.where(
        (padded_docs[1 : length + 1] == doc_ids)[:, None], padded[1 : length + 1], 0.0
    )
    two_back = jnp.where((padded_docs[:length] == doc_ids)[:, None], padded[:length], 0.0)
    mixed_rows = tap_values[2] * inner_prod + tap_values[1] * one_back + tap_values[0] * two_back
    conv_out = (gate_outer.astype(jnp.float32) * mixed_rows).astype(jnp.bfloat16)
    row_count = residual_in.shape[0]
    regrouped = lax.all_to_all(conv_out, "tp", split_axis=0, concat_axis=1, tiled=True)
    mix = jnp.dot(regrouped, out_proj, preferred_element_type=jnp.float32).astype(jnp.bfloat16)
    carried = residual_in.astype(jnp.float32) + mix.astype(jnp.float32)
    normed = (
        carried * lax.rsqrt(jnp.mean(carried * carried, axis=1, keepdims=True) + 1e-06) * norm_gain
    ).astype(jnp.bfloat16)
    model_width = normed.shape[1]
    choose = expert_ids.shape[1]
    sp_count = lax.axis_size("sp")
    tp_count = lax.axis_size("tp")
    experts_total = sp_count * tp_count
    capacity = 2 * row_count * choose // experts_total
    flat_ids = expert_ids.reshape(-1)
    onehot = (flat_ids[:, None] == jnp.arange(experts_total, dtype=jnp.int32)[None, :]).astype(
        jnp.int32
    )
    slot_rank = jnp.sum((jnp.cumsum(onehot, axis=0) - 1) * onehot, axis=1)
    target = flat_ids * capacity + slot_rank
    sources = jnp.repeat(normed, choose, axis=0)
    outgoing = (
        jnp.zeros((experts_total * capacity, model_width), jnp.bfloat16).at[target].set(sources)
    )
    gate_weight = gate_proj[0]
    up_weight = up_proj[0]
    down_weight = down_proj[0]
    arrived = lax.all_to_all(
        outgoing.reshape(experts_total, capacity, model_width),
        ("sp", "tp"),
        split_axis=0,
        concat_axis=0,
        tiled=True,
    )
    item_count = arrived.shape[1]
    flat_rows = arrived.reshape(-1, model_width)
    result = expert_rows(flat_rows, gate_weight, up_weight, down_weight)
    result = result.reshape(experts_total, item_count, model_width)
    returned = lax.all_to_all(result, ("sp", "tp"), split_axis=0, concat_axis=0, tiled=True)
    picked = (
        returned.reshape(-1, model_width)[target]
        .reshape(row_count, choose, model_width)
        .astype(jnp.float32)
    )
    combined = carried + jnp.sum(expert_weights[:, :, None] * picked, axis=1)
    return combined.astype(jnp.bfloat16)


def solution(mesh):
    in_specs = (
        P("sp", "tp"),
        P("sp", "tp"),
        P("sp", "tp"),
        P(None, "tp"),
        P("sp"),
        P(("sp", "tp"), None),
        P(),
        P(),
        P(("sp", "tp"), None),
        P(("sp", "tp"), None),
        P(("sp", "tp"), None, None),
        P(("sp", "tp"), None, None),
        P(("sp", "tp"), None, None),
    )
    out_specs = P(("sp", "tp"), None)
    return jax.shard_map(
        on_device, mesh=mesh, in_specs=in_specs, out_specs=out_specs, check_vma=False
    )
```

profile of v0, /device:TPU:1, one launch (start us, length us, event | category | flops | bytes accessed | tf_op | source)
XLA Modules:
  0.0 143.9 jit_solution(9995977291659634800)
XLA Ops:
  0.0 1.2 convert_multiply_fusion
  1.2 4.6 %collective-permute-start.1 = (f32[2,256]{1,0:T(2,128)S(1)}, f32[2,256]{1,0:T(2,128)S(1)}, u32[]{:S(2)}, u32[]{:S(2)}) collective-permute-start(f32[2,256]{1,0:T(2,128)S(1)} %slice.48), channel_id=1, source_target_pairs={{0,4},{4,8},{8,12},{12,16},{16,20},{20,24},{24,28},{28,32},{32,36}... | collective-permute-start | bytes 6152 | tf_op jit(solution)/shard_map/ppermute | solution.py:10
  5.8 0.8 slice.35
  6.5 1.9 %collective-permute-start = (s32[2]{0:T(128)S(1)}, s32[2]{0:T(128)S(1)}, u32[]{:S(2)}, u32[]{:S(2)}) collective-permute-start(s32[2]{0:T(128)S(1)} %slice.35), channel_id=1, source_target_pairs={{0,4},{4,8},{8,12},{12,16},{16,20},{20,24},{24,28},{28,32},{32,36}... | collective-permute-start | bytes 32 | tf_op jit(solution)/shard_map/ppermute | solution.py:10
  8.4 0.8 copy.24
  9.4 0.1 eq.33
  9.5 0.7 broadcast_multiply_fusion
  10.2 0.8 fusion.31
  11.1 0.2 fusion.26
  11.7 0.2 fusion.27
  12.1 1.0 fusion.23
  13.1 4.0 %all-to-all-start = ((bf16[4,128,256]{2,1,0:T(8,128)(2,1)}), bf16[4,128,256]{2,1,0:T(8,128)(2,1)S(1)}, u32[]{:S(2)}, u32[]{:S(2)}) async-start(bf16[4,128,256]{2,1,0:T(8,128)(2,1)} %bitcast.3), calls=%async_computation | async-start | bytes 524288 | tf_op jit(solution)/shard_map/all_to_all | solution.py:48
  17.1 5.7 %all-to-all-done = bf16[4,128,256]{2,1,0:T(8,128)(2,1)S(1)} async-done(((bf16[4,128,256]{2,1,0:T(8,128)(2,1)}), bf16[4,128,256]{2,1,0:T(8,128)(2,1)S(1)}, u32[]{:S(2)}, u32[]{:S(2)}) %all-to-all-start) | async-done | bytes 262176 | tf_op jit(solution)/shard_map/all_to_all | solution.py:48
  22.8 0.2 copy.21
  23.0 3.0 %multiply_reduce_fusion.1 = (f32[128]{0:T(128)S(1)}, f32[128,2048]{1,0:T(8,128)S(1)}) fusion(bf16[128,1024]{0,1:T(8,128)(2,1)S(1)} %bitcast.35, bf16[1024,2048]{1,0:T(8,128)(2,1)} %param.19, bf16[128,2048]{1,0:T(8,128)(2,1)S(1)} %copy-done.1), kind=kOutput, calls=%fused_computation.16 | convolution fusion | flops 538443648 | bytes 6029824 | tf_op jit(solution)/shard_map/dot_general | solution.py:49
  26.0 0.2 multiply_convert_fusion.1
  26.2 0.6 broadcast_in_dim.36
  26.8 1.2 reshape.100
  28.1 3.5 %scatter_custom_fusion = bf16[512,2048]{1,0:T(8,128)(2,1)S(1)} fusion(s32[256]{0:T(256)S(1)} %bitcast.38, bf16[256,2048]{1,0:T(8,128)(2,1)} %reshape.100, bf16[]{:T(256)} %constant.6.clone.1), kind=kCustom, calls=%fused_computation.17 | custom fusion | bytes 2097664 | tf_op jit(solution)/shard_map/scatter | solution.py:68
  31.6 2.2 %reshape.83 = bf16[128,4,2048]{2,1,0:T(4,128)(2,1)} reshape(bf16[512,2048]{1,0:T(8,128)(2,1)S(1)} %scatter_custom_fusion) | data formatting | bytes 4194304 | tf_op jit(solution)/shard_map/reshape | solution.py:74
  33.8 40.5 %all_to_all.29 = bf16[128,4,2048]{2,1,0:T(4,128)(2,1)S(1)} all-to-all(bf16[128,4,2048]{2,1,0:T(4,128)(2,1)} %reshape.83), channel_id=1, replica_groups=mesh['sp'=32,'tp'=4] {'sp','tp'}, dimensions={0} | all-to-all | bytes 4194304 | tf_op jit(solution)/shard_map/all_to_all | solution.py:73
  74.3 2.0 %reshape.84 = bf16[512,2048]{1,0:T(8,128)(2,1)} reshape(bf16[128,4,2048]{2,1,0:T(4,128)(2,1)S(1)} %all_to_all.29) | data formatting | bytes 4194304 | tf_op jit(solution)/shard_map/reshape | solution.py:81
  76.4 6.6 %fusion.4 = f32[512,1024]{1,0:T(8,128)} fusion(bf16[512,2048]{1,0:T(8,128)(2,1)} %reshape.84, bf16[1,2048,1024]{2,1,0:T(8,128)(2,1)} %param.23), kind=kOutput, calls=%fused_computation.6 | convolution fusion | flops 2147483648 | bytes 8388608 | tf_op jit(solution)/shard_map/dot_general | solution.py:14
  83.0 9.9 %fusion.6 = bf16[512,2048]{1,0:T(8,128)(2,1)} fusion(bf16[1,1024,2048]{2,1,0:T(8,128)(2,1)} %param.25, f32[512,1024]{1,0:T(8,128)} %fusion.4, bf16[512,2048]{1,0:T(8,128)(2,1)S(1)} %copy-done, bf16[1,2048,1024]{2,1,0:T(8,128)(2,1)} %param.24), kind=kOutput, calls=%fused_computation.8 | convolution fusion | flops 4299161600 | bytes 14680064 | tf_op jit(solution)/shard_map/dot_general | solution.py:17
  92.9 4.1 %reshape.85 = bf16[128,4,2048]{2,1,0:T(4,128)(2,1)} reshape(bf16[512,2048]{1,0:T(8,128)(2,1)} %fusion.6) | data formatting | bytes 4194304 | tf_op jit(solution)/shard_map/reshape | solution.py:83
  97.0 5.0 %all-to-all-start.2 = ((bf16[128,4,2048]{2,1,0:T(4,128)(2,1)}), bf16[128,4,2048]{2,1,0:T(4,128)(2,1)}, u32[]{:S(2)}, u32[]{:S(2)}) async-start(bf16[128,4,2048]{2,1,0:T(4,128)(2,1)} %reshape.85), calls=%async_computation.2 | async-start | bytes 4194304 | tf_op jit(solution)/shard_map/all_to_all | solution.py:84
  102.1 30.4 %all-to-all-done.2 = bf16[128,4,2048]{2,1,0:T(4,128)(2,1)} async-done(((bf16[128,4,2048]{2,1,0:T(4,128)(2,1)}), bf16[128,4,2048]{2,1,0:T(4,128)(2,1)}, u32[]{:S(2)}, u32[]{:S(2)}) %all-to-all-start.2) | async-done | bytes 2097184 | tf_op jit(solution)/shard_map/all_to_all | solution.py:84
  132.6 2.5 %reshape.86 = bf16[512,2048]{1,0:T(8,128)(2,1)S(1)} reshape(bf16[128,4,2048]{2,1,0:T(4,128)(2,1)} %all-to-all-done.2) | data formatting | bytes 4194304 | tf_op jit(solution)/shard_map/reshape | solution.py:86
  135.1 2.3 %gather_fusion = bf16[256,2048]{1,0:T(8,128)(2,1)} fusion(bf16[512,2048]{1,0:T(8,128)(2,1)S(1)} %reshape.86, s32[1024]{0:T(1024)S(1)} %pad_clamp_fusion), kind=kCustom, calls=%fused_computation | custom fusion | bytes 2098176 | tf_op jit(solution)/shard_map/gather | solution.py:86
  137.4 2.4 %reshape.87 = f32[128,2,2048]{2,1,0:T(2,128)S(1)} reshape(bf16[256,2048]{1,0:T(8,128)(2,1)} %gather_fusion) | data formatting | bytes 3145728 | tf_op jit(solution)/shard_map/convert_element_type | solution.py:88
  139.8 3.2 %multiply_reduce_fusion = f32[128,2048]{1,0:T(8,128)S(1)} fusion(f32[128,2,2048]{2,1,0:T(2,128)S(1)} %reshape.87, f32[128,2]{1,0:T(8,128)S(1)} %copy.22), kind=kLoop, calls=%fused_computation.12 | loop fusion | flops 786432 | bytes 3146752 | tf_op jit(solution)/shard_map/reduce_sum | solution.py:90
  143.0 0.9 add_convert_fusion
  (30 shorter events, 0.9 us)
Async XLA Ops:
  0.0 11.9 %copy-start.4 = (s32[512]{0:T(512)S(1)}, s32[512]{0:T(512)}, u32[]{:S(2)}) copy-start(s32[512]{0:T(512)} %param.17) | copy-start | bytes 6148
  0.0 12.1 %copy-start.2 = (bf16[512,256]{1,0:T(8,128)(2,1)S(1)}, bf16[512,256]{1,0:T(8,128)(2,1)}, u32[]{:S(2)}) copy-start(bf16[512,256]{1,0:T(8,128)(2,1)} %param.15) | copy-start | bytes 786436
  0.0 23.0 %copy-start.1 = (bf16[128,2048]{1,0:T(8,128)(2,1)S(1)}, bf16[128,2048]{1,0:T(8,128)(2,1)}, u32[]{:S(2)}) copy-start(bf16[128,2048]{1,0:T(8,128)(2,1)} %param.18) | copy-start | bytes 1572868
  1.2 10.9 %collective-permute-start.1 = (f32[2,256]{1,0:T(2,128)S(1)}, f32[2,256]{1,0:T(2,128)S(1)}, u32[]{:S(2)}, u32[]{:S(2)}) collective-permute-start(f32[2,256]{1,0:T(2,128)S(1)} %slice.48), channel_id=1, source_target_pairs={{0,4},{4,8},{8,12},{12,16},{16,20},{20,24},{24,28},{28,32},{32,36}... | collective-permute-start | bytes 6152 | tf_op jit(solution)/shard_map/ppermute | solution.py:10
  6.5 5.4 %collective-permute-start = (s32[2]{0:T(128)S(1)}, s32[2]{0:T(128)S(1)}, u32[]{:S(2)}, u32[]{:S(2)}) collective-permute-start(s32[2]{0:T(128)S(1)} %slice.35), channel_id=1, source_target_pairs={{0,4},{4,8},{8,12},{12,16},{16,20},{20,24},{24,28},{28,32},{32,36}... | collective-permute-start | bytes 32 | tf_op jit(solution)/shard_map/ppermute | solution.py:10
  13.1 9.7 %all-to-all-start = ((bf16[4,128,256]{2,1,0:T(8,128)(2,1)}), bf16[4,128,256]{2,1,0:T(8,128)(2,1)S(1)}, u32[]{:S(2)}, u32[]{:S(2)}) async-start(bf16[4,128,256]{2,1,0:T(8,128)(2,1)} %bitcast.3), calls=%async_computation | async-start | bytes 524288 | tf_op jit(solution)/shard_map/all_to_all | solution.py:48
  23.0 3.0 %copy-start.3 = (f32[2048]{0:T(1024)S(1)}, f32[2048]{0:T(1024)}, u32[]{:S(2)}) copy-start(f32[2048]{0:T(1024)} %param.20) | copy-start | bytes 24580
  76.4 6.7 %copy-start = (bf16[512,2048]{1,0:T(8,128)(2,1)S(1)}, bf16[512,2048]{1,0:T(8,128)(2,1)}, u32[]{:S(2)}) copy-start(bf16[512,2048]{1,0:T(8,128)(2,1)} %reshape.84) | copy-start | bytes 6291460
  97.0 5.0 %copy-start.5 = (f32[128,2]{0,1:T(2,128)S(1)}, f32[128,2]{0,1:T(2,128)}, u32[]{:S(2)}) copy-start(f32[128,2]{0,1:T(2,128)} %param.22) | copy-start | bytes 3076
  97.0 35.5 %all-to-all-start.2 = ((bf16[128,4,2048]{2,1,0:T(4,128)(2,1)}), bf16[128,4,2048]{2,1,0:T(4,128)(2,1)}, u32[]{:S(2)}, u32[]{:S(2)}) async-start(bf16[128,4,2048]{2,1,0:T(4,128)(2,1)} %reshape.85), calls=%async_computation.2 | async-start | bytes 4194304 | tf_op jit(solution)/shard_map/all_to_all | solution.py:84
where the time goes:
time: 145 us; the launch traced here: 144 us
  blocking collectives  40.5 us (28%)
  waiting for transfers between devices  36.1 us (25%)
  local copies, waits for them, and re-layouts  24.3 us (17%)
  matrix products  19.6 us (14%)
  starting transfers between devices  15.5 us (11%)
  other arithmetic  7.76 us (5%)
    all_to_all x1, blocking collectives, on_device(): lax.all_to_all(outgoing.reshape(experts_total, capacity, model_width), ('...  40.5 us
    all_to_all x1, waiting for transfers between devices, on_device(): lax.all_to_all(result, ('sp', 'tp'), split_axis=0, concat_axis=0, tiled=T...  30.4 us
    dot_general x1, matrix products, expert_rows(): jnp.dot(hidden, down_weight, preferred_element_type=jnp.float32)  9.9 us
    dot_general x1, matrix products, expert_rows(): jnp.dot(arrived, gate_weight, preferred_element_type=jnp.float32)  6.65 us
    ppermute x2, starting transfers between devices, from_behind(): return lax.ppermute(block, axis, route)  6.49 us
    all_to_all x1, waiting for transfers between devices, on_device(): lax.all_to_all(conv_out, 'tp', split_axis=0, concat_axis=1, tiled=True)  5.69 us
    all_to_all x1, starting transfers between devices, on_device(): lax.all_to_all(result, ('sp', 'tp'), split_axis=0, concat_axis=0, tiled=T...  4.97 us
    reshape x1, local copies, waits for them, and re-layouts, on_device(): result = result.reshape(experts_total, item_count, model_width)  4.11 us
  transfers between devices with their start and end apart: 4, of which 2 were waited for; matrix products, arithmetic and copies ran while one was open for 3% of the time, Pallas kernels for 0%

commit v1 on v0

v1 whole, which is shorter than its diff:
```python
import functools
import jax
import jax.numpy as jnp
from jax import lax
from jax.experimental import pallas as pl
from jax.experimental.pallas import tpu as pltpu
from jax.sharding import PartitionSpec as P

F32 = jnp.float32
BF16 = jnp.bfloat16
VM = pl.BlockSpec(memory_space=pltpu.VMEM)
SM = pl.BlockSpec(memory_space=pltpu.SMEM)
ANY = pl.BlockSpec(memory_space=pl.ANY)


def dot(a, b):
    return jnp.dot(a, b, preferred_element_type=F32)


def conv_kernel(place, earlier, x, g_in, g_out, taps, docs, o0, o1, o2, o3, prod, doc_col):
    rows = x.shape[0]
    part = o0.shape[0]
    prod[0:8, :] = jnp.concatenate([jnp.zeros((6, x.shape[1]), F32), earlier[0:2, :]], axis=0)
    prod[8:, :] = x[...].astype(F32) * g_in[...].astype(F32)
    doc_col[0:8, :] = jnp.concatenate(
        [jnp.zeros((6, 128), F32), earlier[2:4, 0:128]], axis=0
    )
    for block in range(rows // 128):
        line = jnp.broadcast_to(docs[block : block + 1, :].astype(F32), (128, 128))
        doc_col[8 + 128 * block : 136 + 128 * block, :] = line.T
    t0 = taps[0:1, :].astype(F32)
    t1 = taps[1:2, :].astype(F32)
    t2 = taps[2:3, :].astype(F32)
    here = place[0]
    for shift, out in enumerate((o0, o1, o2, o3)):
        start = pl.multiple_of(lax.rem(here + shift, 4) * part, part)
        window = prod[pl.ds(start, part + 8), :]
        ids = doc_col[pl.ds(start, part + 8), :]
        cur = ids[8:]
        same1 = ids[7:-1] == cur
        same2 = ids[6:-2] == cur
        for half in range(x.shape[1] // 128):
            c = slice(128 * half, 128 * half + 128)
            back1 = jnp.where(same1, window[7:-1, c], 0.0)
            back2 = jnp.where(same2, window[6:-2, c], 0.0)
            mixed = t2[:, c] * window[8:, c] + t1[:, c] * back1 + t0[:, c] * back2
            out[:, c] = (g_out[pl.ds(start, part), c].astype(F32) * mixed).astype(BF16)


def slots_kernel(ids, tgt):
    tokens = ids.shape[1]
    first = ids[0:1, :]
    second = ids[1:2, :]
    expert = lax.broadcasted_iota(jnp.int32, (128, tokens), 0)
    m0 = (expert == first).astype(F32)
    m1 = (expert == second).astype(F32)
    r = lax.broadcasted_iota(jnp.int32, (tokens, tokens), 0)
    c = lax.broadcasted_iota(jnp.int32, (tokens, tokens), 1)
    before = (r < c).astype(BF16)
    n0 = dot(m0.astype(BF16), before)
    n1 = dot(m1.astype(BF16), before) + jnp.sum(m0, axis=1, keepdims=True)
    rank0 = jnp.sum(m0 * n0, axis=0, keepdims=True).astype(jnp.int32)
    rank1 = jnp.sum(m1 * n1, axis=0, keepdims=True).astype(jnp.int32)
    tgt[0:1, :] = first * 8 + rank0
    tgt[1:2, :] = second * 8 + rank1


def mix_kernel(place, r0, r1, r2, r3, residual, proj, gain, tgt, buf, carried, halves, onehot):
    here = place[0]
    width = residual.shape[1]
    half = width // 2
    tokens = residual.shape[0]
    row = lax.broadcasted_iota(jnp.int32, (buf.shape[0], tokens), 0)
    a, b = tgt[0:1, :], tgt[1:2, :]
    onehot[:, 0:tokens] = ((row == a) | (row == b)).astype(F32).astype(BF16)
    onehot[:, tokens:] = ((row == a + 4) | (row == b + 4)).astype(F32).astype(BF16)
    step = 512
    total = jnp.zeros((tokens, 1), F32)
    for n in range(width // step):
        c = slice(n * step, n * step + step)
        acc = None
        for shift, part in enumerate((r0, r1, r2, r3)):
            depth = part.shape[1]
            start = pl.multiple_of(lax.rem(here + 4 - shift, 4) * depth, depth)
            term = dot(part[...], proj[pl.ds(start, depth), c])
            acc = term if acc is None else acc + term
        value = residual[:, c].astype(F32) + acc.astype(BF16).astype(F32)
        carried[:, c] = value
        total = total + jnp.sum(value * value, axis=1, keepdims=True)
    scale = lax.rsqrt(total * (1.0 / width) + 1e-06)
    for n in range(width // step):
        c = slice(n * step, n * step + step)
        value = (carried[:, c] * scale * gain[:, c]).astype(BF16)
        h = (n * step) // half
        halves[h * tokens : (h + 1) * tokens, n * step - h * half : n * step - h * half + step] = value
    for n in range(half // 256):
        c = slice(n * 256, n * 256 + 256)
        buf[:, c] = dot(onehot[...], halves[:, c]).astype(BF16)


def expert_kernel(arrived, wg, wu, wd, out, av, gv, uv, dv, xv, hv, ov, sem_a, sem_g, sem_u, sem_d, sem_o):
    rows, half = av.shape
    depth, hidden = gv.shape
    blocks = hidden // 256
    cols = [slice(256 * j, 256 * j + 256) for j in range(blocks)]
    copies_a = [pltpu.make_async_copy(arrived.at[:, c], av.at[:, c], sem_a.at[j]) for j, c in enumerate(cols)]
    copies_g = [pltpu.make_async_copy(wg.at[:, c], gv.at[:, c], sem_g.at[j]) for j, c in enumerate(cols)]
    copies_u = [pltpu.make_async_copy(wu.at[:, c], uv.at[:, c], sem_u.at[j]) for j, c in enumerate(cols)]
    cols_d = [slice(512 * j, 512 * j + 512) for j in range(blocks)]
    copies_d = [pltpu.make_async_copy(wd.at[:, c], dv.at[:, c], sem_d.at[j]) for j, c in enumerate((cols_d[0], cols_d[2], cols_d[1], cols_d[3]))]
    for copy in copies_a:
        copy.start()
    for a, b in zip(copies_g, copies_u):
        a.start()
        b.start()
    for copy in copies_d:
        copy.start()
    low = lax.broadcasted_iota(jnp.int32, (rows // 16, 8, 256), 1) < 4
    for j, c in enumerate(cols):
        copies_a[j].wait()
        value = av[:, c].astype(F32).reshape(rows // 16, 2, 8, 256)
        even, odd = value[:, 0], value[:, 1]
        lo = jnp.where(low, even, pltpu.roll(odd, 4, 1))
        hi = jnp.where(low, pltpu.roll(even, 4, 1), odd)
        xv[:, c] = lo.reshape(rows // 2, 256).astype(BF16)
        xv[:, half + 256 * j : half + 256 * j + 256] = hi.reshape(rows // 2, 256).astype(BF16)
    for j, c in enumerate(cols):
        copies_g[j].wait()
        copies_u[j].wait()
        gate = dot(xv[...], gv[:, c])
        up = dot(xv[...], uv[:, c])
        hv[:, c] = (gate / (1.0 + jnp.exp(-gate)) * up).astype(BF16)
    outs = []
    for j, c in enumerate(cols):
        if j % 2 == 0:
            copies_d[j].wait()
            copies_d[j + 1].wait()
        lo = dot(hv[...], dv[:, c]).reshape(rows // 16, 8, 256)
        hi = dot(hv[...], dv[:, half + 256 * j : half + 256 * j + 256]).reshape(rows // 16, 8, 256)
        even = jnp.where(low, lo, pltpu.roll(hi, 4, 1))
        odd = jnp.where(low, pltpu.roll(lo, 4, 1), hi)
        ov[:, c] = jnp.stack([even, odd], axis=1).reshape(rows, 256).astype(BF16)
        copy = pltpu.make_async_copy(ov.at[:, c], out.at[:, c], sem_o.at[j])
        copy.start()
        outs.append(copy)
    for copy in outs:
        copy.wait()


def combine_kernel(returned, carried, tgt, weights, out, pick):
    tokens = carried.shape[0]
    rows, half = returned.shape
    for k in range(2):
        line = jnp.broadcast_to(tgt[k : k + 1, :].astype(F32), (128, tokens)).T
        for n in range(rows // 128):
            lane = (lax.broadcasted_iota(jnp.int32, (tokens, 128), 1) + 128 * n).astype(F32)
            c = slice(128 * n, 128 * n + 128)
            pick[0, k * tokens : (k + 1) * tokens, c] = (line == lane).astype(F32).astype(BF16)
            pick[1, k * tokens : (k + 1) * tokens, c] = (line + 4.0 == lane).astype(F32).astype(BF16)
    w = [jnp.broadcast_to(weights[k : k + 1, :], (128, tokens)).T[:, 0:1] for k in range(2)]
    for h in range(2):
        for n in range(half // 256):
            c = slice(256 * n, 256 * n + 256)
            d = slice(h * half + 256 * n, h * half + 256 * n + 256)
            both = dot(pick[h], returned[:, c])
            out[:, d] = (carried[:, d] + (w[0] * both[:tokens] + w[1] * both[tokens:])).astype(BF16)


def call(kernel, out_shape, in_specs, out_specs, scratch, vmem_mib, flops=0, nbytes=0, name=None):
    return pl.pallas_call(
        kernel,
        out_shape=out_shape,
        in_specs=in_specs,
        out_specs=out_specs,
        scratch_shapes=scratch,
        name=name,
        compiler_params=pltpu.CompilerParams(vmem_limit_bytes=vmem_mib << 20),
        cost_estimate=pl.CostEstimate(flops=flops, bytes_accessed=nbytes, transcendentals=0),
    )


def shape(dims, kind):
    return jax.ShapeDtypeStruct(dims, kind)


def on_device(conv_input, gate_inner, gate_outer, conv_taps, doc_ids, residual_in, out_proj,
              norm_gain, expert_ids, expert_weights, gate_proj, up_proj, down_proj):
    length, channels = conv_input.shape
    tokens, width = residual_in.shape
    sp_count = lax.axis_size("sp")
    tp_count = lax.axis_size("tp")
    experts = sp_count * tp_count
    place = lax.axis_index("tp").reshape(1)
    tail = conv_input[-2:].astype(F32) * gate_inner[-2:].astype(F32)
    tail_docs = jnp.broadcast_to(doc_ids[-2:].astype(F32)[:, None], (2, channels))
    earlier = lax.ppermute(
        jnp.concatenate([tail, tail_docs], axis=0), "sp", [(i, i + 1) for i in range(sp_count - 1)]
    )
    tgt = call(
        slots_kernel, shape((2, tokens), jnp.int32), [VM], VM, [], 8, 1 << 22, 1 << 16, name="slots"
    )(expert_ids.T)
    piece = shape((tokens, channels), BF16)
    sent = call(
        conv_kernel, (piece,) * 4, [SM] + [VM] * 6, (VM,) * 4,
        [pltpu.VMEM((length + 8, channels), F32), pltpu.VMEM((length + 8, 128), F32)],
        16, 1 << 22, 1 << 20, name="conv",
    )(place, earlier, conv_input, gate_inner, gate_outer, conv_taps, doc_ids.reshape(-1, 128))
    parts = [sent[0]] + [
        lax.ppermute(sent[d], "tp", [(i, (i + d) % tp_count) for i in range(tp_count)])
        for d in range(1, tp_count)
    ]
    rows = experts * 8
    half = width // 2
    buf, carried = call(
        mix_kernel, (shape((rows, half), BF16), shape((tokens, width), F32)),
        [SM] + [VM] * 8, (VM, VM),
        [pltpu.VMEM((2 * tokens, half), BF16), pltpu.VMEM((rows, 2 * tokens), BF16)],
        32, 1 << 30, 1 << 23, name="mix",
    )(place, *parts, residual_in, out_proj, norm_gain.reshape(1, -1), tgt)
    arrived = lax.all_to_all(buf.reshape(experts, 8, half), ("sp", "tp"), split_axis=0, concat_axis=0, tiled=True)
    hidden = gate_proj.shape[2]
    dma = pltpu.SemaphoreType.DMA((hidden // 256,))
    result = call(
        expert_kernel, shape((rows, half), BF16), [ANY] * 4, ANY,
        [
            pltpu.VMEM((rows, half), BF16),
            pltpu.VMEM((width, hidden), BF16),
            pltpu.VMEM((width, hidden), BF16),
            pltpu.VMEM((hidden, width), BF16),
            pltpu.VMEM((rows // 2, width), BF16),
            pltpu.VMEM((rows // 2, hidden), BF16),
            pltpu.VMEM((rows, half), BF16),
        ] + [dma] * 5,
        48, 6 << 30, 1 << 24, name="experts",
    )(arrived.reshape(rows, half), gate_proj[0], up_proj[0], down_proj[0])
    returned = lax.all_to_all(result.reshape(experts, 8, half), ("sp", "tp"), split_axis=0, concat_axis=0, tiled=True)
    return call(
        combine_kernel, shape((tokens, width), BF16), [VM] * 4, VM,
        [pltpu.VMEM((2, 2 * tokens, rows), BF16)],
        32, 1 << 30, 1 << 22, name="combine",
    )(returned.reshape(rows, half), carried, tgt, expert_weights.T)


def solution(mesh):
    both = ("sp", "tp")
    in_specs = (
        P("sp", "tp"),
        P("sp", "tp"),
        P("sp", "tp"),
        P(None, "tp"),
        P("sp"),
        P(both, None),
        P(),
        P(),
        P(both, None),
        P(both, None),
        P(both, None, None),
        P(both, None, None),
        P(both, None, None),
    )
    return jax.shard_map(
        on_device, mesh=mesh, in_specs=in_specs, out_specs=P(both, None), check_vma=False
    )
```

time: 145 us -> 114 us (0.79)
  blocking collectives: 40.5 us -> 76.7 us
  waiting for transfers between devices: 36.1 us -> 2.32 us
  matrix products: 19.6 us -> 0 us
  local copies, waits for them, and re-layouts: 24.3 us -> 8.9 us
  Pallas kernels: 0 us -> 14.9 us
  other arithmetic: 7.76 us -> 1.53 us
  starting transfers between devices: 15.5 us -> 9.47 us
    all_to_all x1 -> x2, blocking collectives: 40.5 us -> 76.7 us  [the longest x1 42.5 us: on_device(): lax.all_to_all(buf.reshape(experts, 8, half), ('sp', 'tp'), split_axis=0,...]
    all_to_all x2 -> x0, waiting for transfers between devices: 36.1 us -> none  [the longest x1 30.4 us: on_device(): lax.all_to_all(result, ('sp', 'tp'), split_axis=0, concat_axis=0, tiled=T...]
    dot_general x3 -> x0, matrix products: 19.6 us -> none  [the longest x1 9.9 us: expert_rows(): jnp.dot(hidden, down_weight, preferred_element_type=jnp.float32)]
    pallas_call x0 -> x5, Pallas kernels: none -> 14.9 us  [the longest x1 10.3 us: on_device(): call(expert_kernel, shape((rows, half), BF16), [ANY] * 4, ANY, [pltpu.VME...]
    reshape x5 -> x0, local copies, waits for them, and re-layouts: 12.1 us -> none  [the longest x1 4.11 us: on_device(): result = result.reshape(experts_total, item_count, model_width)]
    all_to_all x2 -> x0, starting transfers between devices: 8.99 us -> none  [the longest x1 4.97 us: on_device(): lax.all_to_all(result, ('sp', 'tp'), split_axis=0, concat_axis=0, tiled=T...]
    unnamed x14 -> x20, local copies, waits for them, and re-layouts: 0.93 us -> 8.82 us
    scatter x1 -> x0, local copies, waits for them, and re-layouts: 3.5 us -> none  [on_device(): jnp.zeros((experts_total * capacity, model_width), jnp.bfloat16).at[target]]
  transfers between devices with their start and end apart: 4 -> 4, of which waited for: 2 -> 3; matrix products, arithmetic and copies ran while one was open for 3% -> 0% of each run, Pallas kernels for 0% -> 0%
where the time goes in v1:
time: 114 us
  blocking collectives  76.7 us (67%)
  Pallas kernels  14.9 us (13%)
  starting transfers between devices  9.47 us (8%)
  local copies, waits for them, and re-layouts  8.9 us (8%)
  waiting for transfers between devices  2.32 us (2%)
  other arithmetic  1.53 us (1%)
    all_to_all x1, blocking collectives, on_device(): lax.all_to_all(buf.reshape(experts, 8, half), ('sp', 'tp'), split_axis=0,...  42.5 us
    all_to_all x1, blocking collectives, on_device(): lax.all_to_all(result.reshape(experts, 8, half), ('sp', 'tp'), split_axis...  34.2 us
    pallas_call x1, Pallas kernels, on_device(): call(expert_kernel, shape((rows, half), BF16), [ANY] * 4, ANY, [pltpu.VME...  10.3 us
    unnamed x20, local copies, waits for them, and re-layouts  8.82 us
    ppermute x3, starting transfers between devices, on_device(): lax.ppermute(sent[d], 'tp', [(i, (i + d) % tp_count) for i in range(tp_co...  4.89 us
    ppermute x1, starting transfers between devices, on_device(): lax.ppermute(jnp.concatenate([tail, tail_docs], axis=0), 'sp', [(i, i + 1...  4.57 us
    pallas_call x1, Pallas kernels, on_device(): call(combine_kernel, shape((tokens, width), BF16), [VM] * 4, VM, [pltpu.V...  2.31 us
  transfers between devices with their start and end apart: 4, of which 3 were waited for; matrix products, arithmetic and copies ran while one was open for 0% of the time, Pallas kernels for 0%

profile of v1, /device:TPU:1, one launch (start us, length us, event | category | flops | bytes accessed | tf_op | source)
XLA Modules:
  0.0 113.9 jit_solution(7548718266462731171)
XLA Ops:
  0.0 0.8 slice_convert_fusion
  0.8 0.1 pad.1.clone
  0.8 0.7 convert_multiply_fusion
  1.5 0.1 pad_maximum_fusion
  1.6 4.6 %collective-permute-start = (f32[4,256]{1,0:T(4,128)S(1)}, f32[4,256]{1,0:T(4,128)S(1)}, u32[]{:S(2)}, u32[]{:S(2)}) collective-permute-start(f32[4,256]{1,0:T(4,128)S(1)} %pad_maximum_fusion), channel_id=1, source_target_pairs={{0,4},{4,8},{8,12},{12,16},{16,20},{20,24},{24,28},{28,32},{32,36}... | collective-permute-start | bytes 12296 | tf_op jit(solution)/shard_map/ppermute | solution.py:196
  6.2 0.7 collective-permute-done.earlier
  6.9 0.0 copy-start.2
  6.9 0.9 copy-done.2
  7.9 0.0 copy-start.3
  7.9 0.9 copy-done.3
  8.8 0.9 copy-done.4
  9.8 0.7 copy-done.6
  10.5 0.7 copy-done.7
  11.1 0.5 conv.1
  11.7 1.3 %collective-permute-start.1 = (bf16[128,256]{1,0:T(8,128)(2,1)S(1)}, bf16[128,256]{1,0:T(8,128)(2,1)S(1)}, u32[]{:S(2)}, u32[]{:S(2)}) collective-permute-start(bf16[128,256]{1,0:T(8,128)(2,1)S(1)} %get-tuple-element.12), channel_id=1, source_target_pairs={{0,1},{1,2},{2,3},{3,0},{4,5},{5,6},{6,7},{7,4},{8,9},{9,10},{10,1... | collective-permute-start | bytes 196616 | tf_op jit(solution)/shard_map/ppermute | solution.py:209
  12.9 2.5 %collective-permute-start.2 = (bf16[128,256]{1,0:T(8,128)(2,1)S(1)}, bf16[128,256]{1,0:T(8,128)(2,1)S(1)}, u32[]{:S(2)}, u32[]{:S(2)}) collective-permute-start(bf16[128,256]{1,0:T(8,128)(2,1)S(1)} %get-tuple-element.13), channel_id=1, source_target_pairs={{0,2},{1,3},{2,0},{3,1},{4,6},{5,7},{6,4},{7,5},{8,10},{9,11},{10,... | collective-permute-start | bytes 196616 | tf_op jit(solution)/shard_map/ppermute | solution.py:209
  15.4 1.1 %collective-permute-start.3 = (bf16[128,256]{1,0:T(8,128)(2,1)S(1)}, bf16[128,256]{1,0:T(8,128)(2,1)S(1)}, u32[]{:S(2)}, u32[]{:S(2)}) collective-permute-start(bf16[128,256]{1,0:T(8,128)(2,1)S(1)} %get-tuple-element.14), channel_id=1, source_target_pairs={{0,3},{1,0},{2,1},{3,2},{4,7},{5,4},{6,5},{7,6},{8,11},{9,8},{10,9... | collective-permute-start | bytes 196616 | tf_op jit(solution)/shard_map/ppermute | solution.py:209
  16.6 0.7 copy-done.8
  17.2 0.2 slots.1.tgt
  17.4 0.0 collective-permute-done.1.r1
  17.4 1.0 collective-permute-done.2.r2
  18.4 0.6 collective-permute-done.3.r3
  19.0 2.2 %copy-done = bf16[1024,2048]{1,0:T(8,128)(2,1)S(1)} copy-done((bf16[1024,2048]{1,0:T(8,128)(2,1)S(1)}, bf16[1024,2048]{1,0:T(8,128)(2,1)}, u32[]{:S(2)}) %copy-start) | copy-done | bytes 4194328
  21.2 1.0 copy-done.1
  22.2 0.7 copy-done.5
  22.9 1.6 %mix.1 = (bf16[1024,1024]{1,0:T(8,128)(2,1)S(1)}, f32[128,2048]{1,0:T(8,128)S(1)}) custom-call(s32[1]{0:T(128)} %bitcast.place, bf16[128,256]{1,0:T(8,128)(2,1)S(1)} %get-tuple-element.11.r0, bf16[128,256]{1,0:T(8,128)(2,1)S(1)} %collective-permute-done.1.r1, bf16[128,256]{1,0:T(8,128)(2,1)S(1)} %collective-permute-done.2.r2, ...), custom_call_target="tpu_custom_call" | custom-call | flops 1073741824 | bytes 8388608 | tf_op jit(solution)/shard_map/mix/pallas_call | solution.py:214
  24.6 42.5 %all_to_all.10 = bf16[128,8,1024]{2,1,0:T(8,128)(2,1)S(1)} all-to-all(bf16[128,8,1024]{2,1,0:T(8,128)(2,1)S(1)} %bitcast.12), channel_id=1, replica_groups=mesh['sp'=32,'tp'=4] {'sp','tp'}, dimensions={0} | all-to-all | bytes 4194304 | tf_op jit(solution)/shard_map/all_to_all | solution.py:220
  67.1 10.3 %experts.1 = bf16[1024,1024]{1,0:T(8,128)(2,1)S(1)} custom-call(bf16[1024,1024]{1,0:T(8,128)(2,1)S(1)} %bitcast.14, bf16[2048,1024]{1,0:T(8,128)(2,1)} %bitcast.20, bf16[2048,1024]{1,0:T(8,128)(2,1)} %bitcast.21, bf16[1024,2048]{1,0:T(8,128)(2,1)} %bitcast.22), custom_call_target="tpu_custom_call" | custom-call | flops 6442450944 | bytes 16777216 | tf_op jit(solution)/shard_map/experts/pallas_call | solution.py:223
  77.4 0.0 copy-start.9
  77.4 34.2 %all_to_all.11 = bf16[128,8,1024]{2,1,0:T(8,128)(2,1)S(1)} all-to-all(bf16[128,8,1024]{2,1,0:T(8,128)(2,1)S(1)} %bitcast.15), channel_id=1, replica_groups=mesh['sp'=32,'tp'=4] {'sp','tp'}, dimensions={0} | all-to-all | bytes 4194304 | tf_op jit(solution)/shard_map/all_to_all | solution.py:236
  111.6 0.0 copy-done.9
  111.6 2.3 %combine.1 = bf16[128,2048]{1,0:T(8,128)(2,1)} custom-call(bf16[1024,1024]{1,0:T(8,128)(2,1)S(1)} %bitcast.13, f32[128,2048]{1,0:T(8,128)S(1)} %get-tuple-element.16.carried, s32[2,128]{1,0:T(2,128)S(1)} %slots.1.tgt, f32[2,128]{1,0:T(2,128)S(1)} %bitcast.19), custom_call_target="tpu_custom_call" | custom-call | flops 1073741824 | bytes 4194304 | tf_op jit(solution)/shard_map/combine/pallas_call | solution.py:237
  (7 shorter events, 0.0 us)
Async XLA Ops:
  1.6 5.3 %collective-permute-start = (f32[4,256]{1,0:T(4,128)S(1)}, f32[4,256]{1,0:T(4,128)S(1)}, u32[]{:S(2)}, u32[]{:S(2)}) collective-permute-start(f32[4,256]{1,0:T(4,128)S(1)} %pad_maximum_fusion), channel_id=1, source_target_pairs={{0,4},{4,8},{8,12},{12,16},{16,20},{20,24},{24,28},{28,32},{32,36}... | collective-permute-start | bytes 12296 | tf_op jit(solution)/shard_map/ppermute | solution.py:196
  6.9 0.9 copy-start.2
  7.9 0.9 copy-start.3
  8.8 0.9 copy-start.4
  9.8 0.7 copy-start.6
  10.5 0.7 copy-start.7
  11.7 5.7 %collective-permute-start.1 = (bf16[128,256]{1,0:T(8,128)(2,1)S(1)}, bf16[128,256]{1,0:T(8,128)(2,1)S(1)}, u32[]{:S(2)}, u32[]{:S(2)}) collective-permute-start(bf16[128,256]{1,0:T(8,128)(2,1)S(1)} %get-tuple-element.12), channel_id=1, source_target_pairs={{0,1},{1,2},{2,3},{3,0},{4,5},{5,6},{6,7},{7,4},{8,9},{9,10},{10,1... | collective-permute-start | bytes 196616 | tf_op jit(solution)/shard_map/ppermute | solution.py:209
  12.9 5.5 %collective-permute-start.2 = (bf16[128,256]{1,0:T(8,128)(2,1)S(1)}, bf16[128,256]{1,0:T(8,128)(2,1)S(1)}, u32[]{:S(2)}, u32[]{:S(2)}) collective-permute-start(bf16[128,256]{1,0:T(8,128)(2,1)S(1)} %get-tuple-element.13), channel_id=1, source_target_pairs={{0,2},{1,3},{2,0},{3,1},{4,6},{5,7},{6,4},{7,5},{8,10},{9,11},{10,... | collective-permute-start | bytes 196616 | tf_op jit(solution)/shard_map/ppermute | solution.py:209
  15.4 3.6 %collective-permute-start.3 = (bf16[128,256]{1,0:T(8,128)(2,1)S(1)}, bf16[128,256]{1,0:T(8,128)(2,1)S(1)}, u32[]{:S(2)}, u32[]{:S(2)}) collective-permute-start(bf16[128,256]{1,0:T(8,128)(2,1)S(1)} %get-tuple-element.14), channel_id=1, source_target_pairs={{0,3},{1,0},{2,1},{3,2},{4,7},{5,4},{6,5},{7,6},{8,11},{9,8},{10,9... | collective-permute-start | bytes 196616 | tf_op jit(solution)/shard_map/ppermute | solution.py:209
  16.6 0.7 copy-start.8
  19.0 2.2 %copy-start = (bf16[1024,2048]{1,0:T(8,128)(2,1)S(1)}, bf16[1024,2048]{1,0:T(8,128)(2,1)}, u32[]{:S(2)}) copy-start(bf16[1024,2048]{1,0:T(8,128)(2,1)} %proj.1) | copy-start | bytes 12582916
  21.2 1.0 copy-start.1
  22.2 0.7 copy-start.5
  77.4 34.2 %copy-start.9 = (f32[128,2]{0,1:T(2,128)S(1)}, f32[128,2]{0,1:T(2,128)}, u32[]{:S(2)}) copy-start(f32[128,2]{0,1:T(2,128)} %param.22) | copy-start | bytes 3076

commit v2 on v1

--- a/solution.py
+++ b/solution.py
@@ -10,11 +10,40 @@
 BF16 = jnp.bfloat16
 VM = pl.BlockSpec(memory_space=pltpu.VMEM)
 SM = pl.BlockSpec(memory_space=pltpu.SMEM)
-ANY = pl.BlockSpec(memory_space=pl.ANY)
+HB = pl.BlockSpec(memory_space=pl.ANY)
 
 
 def dot(a, b):
     return jnp.dot(a, b, preferred_element_type=F32)
+
+
+def edge_kernel(x, g_in, docs, out, xv, gv, dv, sem):
+    rows = x.shape[0]
+    copies = [
+        pltpu.make_async_copy(x.at[rows - 16 :, :], xv, sem.at[0]),
+        pltpu.make_async_copy(g_in.at[rows - 16 :, :], gv, sem.at[1]),
+        pltpu.make_async_copy(docs, dv, sem.at[2]),
+    ]
+    for copy in copies:
+        copy.start()
+    for copy in copies:
+        copy.wait()
+    prod = xv[...].astype(F32) * gv[...].astype(F32)
+    last = dv.shape[0] - 1
+    ids = jnp.broadcast_to(dv[last : last + 1, :].astype(F32), (128, 128)).T
+    out[0:2, :] = prod[14:16, :]
+    for c in range(out.shape[1] // 128):
+        out[2:4, 128 * c : 128 * c + 128] = ids[126:128, :]
+
+
+def load_kernel(*refs):
+    count = (len(refs) - 1) // 2
+    sem = refs[-1]
+    copies = [pltpu.make_async_copy(refs[i], refs[count + i], sem.at[i]) for i in range(count)]
+    for copy in copies:
+        copy.start()
+    for copy in copies:
+        copy.wait()
 
 
 def conv_kernel(place, earlier, x, g_in, g_out, taps, docs, o0, o1, o2, o3, prod, doc_col):
@@ -47,22 +76,33 @@
             out[:, c] = (g_out[pl.ds(start, part), c].astype(F32) * mixed).astype(BF16)
 
 
-def slots_kernel(ids, tgt):
+def slots_kernel(ids, proj, residual, gain, tgt, proj_v, residual_v, gain_v, iv, sem):
+    copies = [
+        pltpu.make_async_copy(ids, iv, sem.at[0]),
+        pltpu.make_async_copy(proj, proj_v, sem.at[1]),
+        pltpu.make_async_copy(residual, residual_v, sem.at[2]),
+        pltpu.make_async_copy(gain, gain_v, sem.at[3]),
+    ]
+    for copy in copies:
+        copy.start()
+    copies[0].wait()
     tokens = ids.shape[1]
-    first = ids[0:1, :]
-    second = ids[1:2, :]
+    first = iv[0:1, :]
+    second = iv[1:2, :]
     expert = lax.broadcasted_iota(jnp.int32, (128, tokens), 0)
     m0 = (expert == first).astype(F32)
     m1 = (expert == second).astype(F32)
     r = lax.broadcasted_iota(jnp.int32, (tokens, tokens), 0)
     c = lax.broadcasted_iota(jnp.int32, (tokens, tokens), 1)
-    before = (r < c).astype(BF16)
+    before = (r < c).astype(F32).astype(BF16)
     n0 = dot(m0.astype(BF16), before)
     n1 = dot(m1.astype(BF16), before) + jnp.sum(m0, axis=1, keepdims=True)
     rank0 = jnp.sum(m0 * n0, axis=0, keepdims=True).astype(jnp.int32)
     rank1 = jnp.sum(m1 * n1, axis=0, keepdims=True).astype(jnp.int32)
     tgt[0:1, :] = first * 8 + rank0
     tgt[1:2, :] = second * 8 + rank1
+    for copy in copies[1:]:
+        copy.wait()
 
 
 def mix_kernel(place, r0, r1, r2, r3, residual, proj, gain, tgt, buf, carried, halves, onehot):
@@ -98,53 +138,37 @@
         buf[:, c] = dot(onehot[...], halves[:, c]).astype(BF16)
 
 
-def expert_kernel(arrived, wg, wu, wd, out, av, gv, uv, dv, xv, hv, ov, sem_a, sem_g, sem_u, sem_d, sem_o):
-    rows, half = av.shape
-    depth, hidden = gv.shape
-    blocks = hidden // 256
+def expert_kernel(arrived, wg, wu, wd, out, dv, xv, hv, sem):
+    rows, half = arrived.shape
+    blocks = wg.shape[1] // 256
     cols = [slice(256 * j, 256 * j + 256) for j in range(blocks)]
-    copies_a = [pltpu.make_async_copy(arrived.at[:, c], av.at[:, c], sem_a.at[j]) for j, c in enumerate(cols)]
-    copies_g = [pltpu.make_async_copy(wg.at[:, c], gv.at[:, c], sem_g.at[j]) for j, c in enumerate(cols)]
-    copies_u = [pltpu.make_async_copy(wu.at[:, c], uv.at[:, c], sem_u.at[j]) for j, c in enumerate(cols)]
-    cols_d = [slice(512 * j, 512 * j + 512) for j in range(blocks)]
-    copies_d = [pltpu.make_async_copy(wd.at[:, c], dv.at[:, c], sem_d.at[j]) for j, c in enumerate((cols_d[0], cols_d[2], cols_d[1], cols_d[3]))]
-    for copy in copies_a:
-        copy.start()
-    for a, b in zip(copies_g, copies_u):
-        a.start()
-        b.start()
-    for copy in copies_d:
+    part = dv.shape[0] // blocks
+    copies = [
+        pltpu.make_async_copy(wd.at[part * j : part * j + part, :], dv.at[part * j : part * j + part, :], sem.at[j])
+        for j in range(blocks)
+    ]
+    for copy in copies:
         copy.start()
     low = lax.broadcasted_iota(jnp.int32, (rows // 16, 8, 256), 1) < 4
     for j, c in enumerate(cols):
-        copies_a[j].wait()
-        value = av[:, c].astype(F32).reshape(rows // 16, 2, 8, 256)
+        value = arrived[:, c].astype(F32).reshape(rows // 16, 2, 8, 256)
         even, odd = value[:, 0], value[:, 1]
         lo = jnp.where(low, even, pltpu.roll(odd, 4, 1))
         hi = jnp.where(low, pltpu.roll(even, 4, 1), odd)
         xv[:, c] = lo.reshape(rows // 2, 256).astype(BF16)
         xv[:, half + 256 * j : half + 256 * j + 256] = hi.reshape(rows // 2, 256).astype(BF16)
     for j, c in enumerate(cols):
-        copies_g[j].wait()
-        copies_u[j].wait()
-        gate = dot(xv[...], gv[:, c])
-        up = dot(xv[...], uv[:, c])
+        gate = dot(xv[...], wg[:, c])
+        up = dot(xv[...], wu[:, c])
         hv[:, c] = (gate / (1.0 + jnp.exp(-gate)) * up).astype(BF16)
-    outs = []
+    for copy in copies:
+        copy.wait()
     for j, c in enumerate(cols):
-        if j % 2 == 0:
-            copies_d[j].wait()
-            copies_d[j + 1].wait()
         lo = dot(hv[...], dv[:, c]).reshape(rows // 16, 8, 256)
         hi = dot(hv[...], dv[:, half + 256 * j : half + 256 * j + 256]).reshape(rows // 16, 8, 256)
         even = jnp.where(low, lo, pltpu.roll(hi, 4, 1))
         odd = jnp.where(low, pltpu.roll(lo, 4, 1), hi)
-        ov[:, c] = jnp.stack([even, odd], axis=1).reshape(rows, 256).astype(BF16)
-        copy = pltpu.make_async_copy(ov.at[:, c], out.at[:, c], sem_o.at[j])
-        copy.start()
-        outs.append(copy)
-    for copy in outs:
-        copy.wait()
+        out[:, c] = jnp.stack([even, odd], axis=1).reshape(rows, 256).astype(BF16)
 
 
 def combine_kernel(returned, carried, tgt, weights, out, pick):
@@ -174,13 +198,22 @@
         out_specs=out_specs,
         scratch_shapes=scratch,
         name=name,
-        compiler_params=pltpu.CompilerParams(vmem_limit_bytes=vmem_mib << 20),
+        compiler_params=pltpu.CompilerParams(vmem_limit_bytes=int(vmem_mib * 1048576)),
         cost_estimate=pl.CostEstimate(flops=flops, bytes_accessed=nbytes, transcendentals=0),
     )
 
 
 def shape(dims, kind):
     return jax.ShapeDtypeStruct(dims, kind)
+
+
+def load(arrays, vmem_mib, name):
+    size = sum(v.size * v.dtype.itemsize for v in arrays)
+    return call(
+        load_kernel, tuple(pltpu.VMEM(v.shape, v.dtype) for v in arrays), [HB] * len(arrays),
+        (VM,) * len(arrays), [pltpu.SemaphoreType.DMA((len(arrays),))], vmem_mib,
+        1 << 30, size, name=name,
+    )(*arrays)
 
 
 def on_device(conv_input, gate_inner, gate_outer, conv_taps, doc_ids, residual_in, out_proj,
@@ -191,53 +224,58 @@
     tp_count = lax.axis_size("tp")
     experts = sp_count * tp_count
     place = lax.axis_index("tp").reshape(1)
-    tail = conv_input[-2:].astype(F32) * gate_inner[-2:].astype(F32)
-    tail_docs = jnp.broadcast_to(doc_ids[-2:].astype(F32)[:, None], (2, channels))
-    earlier = lax.ppermute(
-        jnp.concatenate([tail, tail_docs], axis=0), "sp", [(i, i + 1) for i in range(sp_count - 1)]
-    )
-    tgt = call(
-        slots_kernel, shape((2, tokens), jnp.int32), [VM], VM, [], 8, 1 << 22, 1 << 16, name="slots"
-    )(expert_ids.T)
+    docs = doc_ids.reshape(-1, 128)
+    edge = call(
+        edge_kernel, pltpu.VMEM((4, channels), F32), [HB] * 3, VM,
+        [pltpu.VMEM((16, channels), BF16), pltpu.VMEM((16, channels), BF16),
+         pltpu.VMEM(docs.shape, jnp.int32), pltpu.SemaphoreType.DMA((3,))],
+        63, 1 << 20, 1 << 16, name="edge",
+    )(conv_input, gate_inner, docs)
+    earlier = lax.ppermute(edge, "sp", [(i, i + 1) for i in range(sp_count - 1)])
+    early = load((conv_input, gate_inner, gate_outer, conv_taps, docs), 62, "early")
     piece = shape((tokens, channels), BF16)
     sent = call(
         conv_kernel, (piece,) * 4, [SM] + [VM] * 6, (VM,) * 4,
         [pltpu.VMEM((length + 8, channels), F32), pltpu.VMEM((length + 8, 128), F32)],
         16, 1 << 22, 1 << 20, name="conv",
-    )(place, earlier, conv_input, gate_inner, gate_outer, conv_taps, doc_ids.reshape(-1, 128))
+    )(place, earlier, *early)
     parts = [sent[0]] + [
         lax.ppermute(sent[d], "tp", [(i, (i + d) % tp_count) for i in range(tp_count)])
         for d in range(1, tp_count)
     ]
+    gain = norm_gain.reshape(1, -1)
+    tgt, proj_v, residual_v, gain_v = call(
+        slots_kernel,
+        (pltpu.VMEM((2, tokens), jnp.int32),) + tuple(pltpu.VMEM(v.shape, v.dtype) for v in (out_proj, residual_in, gain)),
+        [HB] * 4, (VM,) * 4,
+        [pltpu.VMEM((2, tokens), jnp.int32), pltpu.SemaphoreType.DMA((4,))],
+        57, 1 << 30, 1 << 23, name="slots",
+    )(expert_ids.T, out_proj, residual_in, gain)
     rows = experts * 8
     half = width // 2
     buf, carried = call(
         mix_kernel, (shape((rows, half), BF16), shape((tokens, width), F32)),
         [SM] + [VM] * 8, (VM, VM),
         [pltpu.VMEM((2 * tokens, half), BF16), pltpu.VMEM((rows, 2 * tokens), BF16)],
-        32, 1 << 30, 1 << 23, name="mix",
-    )(place, *parts, residual_in, out_proj, norm_gain.reshape(1, -1), tgt)
+        24, 1 << 30, 1 << 23, name="mix",
+    )(place, *parts, residual_v, proj_v, gain_v, tgt)
     arrived = lax.all_to_all(buf.reshape(experts, 8, half), ("sp", "tp"), split_axis=0, concat_axis=0, tiled=True)
     hidden = gate_proj.shape[2]
-    dma = pltpu.SemaphoreType.DMA((hidden // 256,))
     result = call(
-        expert_kernel, shape((rows, half), BF16), [ANY] * 4, ANY,
+        expert_kernel, shape((rows, half), BF16), [VM] * 3 + [HB], VM,
         [
-            pltpu.VMEM((rows, half), BF16),
-            pltpu.VMEM((width, hidden), BF16),
-            pltpu.VMEM((width, hidden), BF16),
             pltpu.VMEM((hidden, width), BF16),
             pltpu.VMEM((rows // 2, width), BF16),
             pltpu.VMEM((rows // 2, hidden), BF16),
-            pltpu.VMEM((rows, half), BF16),
-        ] + [dma] * 5,
-        48, 6 << 30, 1 << 24, name="experts",
+            pltpu.SemaphoreType.DMA((hidden // 256,)),
+        ],
+        40, 6 << 30, 1 << 24, name="experts",
     )(arrived.reshape(rows, half), gate_proj[0], up_proj[0], down_proj[0])
     returned = lax.all_to_all(result.reshape(experts, 8, half), ("sp", "tp"), split_axis=0, concat_axis=0, tiled=True)
     return call(
         combine_kernel, shape((tokens, width), BF16), [VM] * 4, VM,
         [pltpu.VMEM((2, 2 * tokens, rows), BF16)],
-        32, 1 << 30, 1 << 22, name="combine",
+        12, 1 << 30, 1 << 22, name="combine",
     )(returned.reshape(rows, half), carried, tgt, expert_weights.T)
 
 

time: 114 us -> 104 us (0.912)
  local copies, waits for them, and re-layouts: 8.9 us -> 0.02 us
  Pallas kernels: 14.9 us -> 17.6 us
  waiting for transfers between devices: 2.32 us -> 0.01 us
  other arithmetic: 1.53 us -> 0 us
    unnamed x20 -> x6, local copies, waits for them, and re-layouts: 8.82 us -> 0.02 us
    pallas_call x2 -> x4, Pallas kernels: 10.5 us -> 13.1 us  [the longest x1 8.74 us: on_device(): call(expert_kernel, shape((rows, half), BF16), [VM] * 3 + [HB], VM, [pltp...]
    ppermute x3, waiting for transfers between devices: 1.59 us -> 0.01 us  [on_device(): lax.ppermute(sent[d], 'tp', [(i, (i + d) % tp_count) for i in range(tp_co...]
  transfers between devices with their start and end apart: 4 -> 4, of which waited for: 3 -> 0; matrix products, arithmetic and copies ran while one was open for 0% -> 0% of each run, Pallas kernels for 0% -> 3%
where the time goes in v2:
time: 104 us; the launch traced here: 103 us
  blocking collectives  76.2 us (73%)
  Pallas kernels  17.6 us (17%)
  starting transfers between devices  9.48 us (9%)
    all_to_all x1, blocking collectives, on_device(): lax.all_to_all(buf.reshape(experts, 8, half), ('sp', 'tp'), split_axis=0,...  42.1 us
    all_to_all x1, blocking collectives, on_device(): lax.all_to_all(result.reshape(experts, 8, half), ('sp', 'tp'), split_axis...  34.2 us
    pallas_call x1, Pallas kernels, on_device(): call(expert_kernel, shape((rows, half), BF16), [VM] * 3 + [HB], VM, [pltp...  8.74 us
    ppermute x3, starting transfers between devices, on_device(): lax.ppermute(sent[d], 'tp', [(i, (i + d) % tp_count) for i in range(tp_co...  4.89 us
    ppermute x1, starting transfers between devices, on_device(): lax.ppermute(edge, 'sp', [(i, i + 1) for i in range(sp_count - 1)])  4.58 us
    pallas_call x1, Pallas kernels, on_device(): call(slots_kernel, (pltpu.VMEM((2, tokens), jnp.int32),) + tuple((pltpu.V...  2.35 us
    pallas_call x1, Pallas kernels, on_device(): call(combine_kernel, shape((tokens, width), BF16), [VM] * 4, VM, [pltpu.V...  2.27 us
  transfers between devices with their start and end apart: 4, of which 0 were waited for; matrix products, arithmetic and copies ran while one was open for 0% of the time, Pallas kernels for 3%

profile of v2, /device:TPU:1, one launch (start us, length us, event | category | flops | bytes accessed | tf_op | source)
XLA Modules:
  0.0 103.4 jit_solution(6785677295798895374)
XLA Ops:
  0.0 0.8 edge.1
  0.9 4.6 %collective-permute-start = (f32[4,256]{1,0:T(4,128)S(1)}, f32[4,256]{1,0:T(4,128)S(1)}, u32[]{:S(2)}, u32[]{:S(2)}) collective-permute-start(f32[4,256]{1,0:T(4,128)S(1)} %edge.1), channel_id=1, source_target_pairs={{0,4},{4,8},{8,12},{12,16},{16,20},{20,24},{24,28},{28,32},{32,36}... | collective-permute-start | bytes 12296 | tf_op jit(solution)/shard_map/ppermute | solution.py:234
  5.4 1.2 %early.1 = (bf16[512,256]{1,0:T(8,128)(2,1)S(1)}, bf16[512,256]{1,0:T(8,128)(2,1)S(1)}, bf16[512,256]{1,0:T(8,128)(2,1)S(1)}, bf16[3,256]{1,0:T(4,128)(2,1)S(1)}, s32[4,128]{1,0:T(4,128)S(1)}) custom-call(bf16[512,256]{1,0:T(8,128)(2,1)} %refs_0_.1, bf16[512,256]{1,0:T(8,128)(2,1)} %refs_1_.1, bf16[512,256]{1,0:T(8,128)(2,1)} %refs_2_.1, ...), custom_call_target="tpu_custom_call" | custom-call | flops 1073741824 | bytes 790016 | tf_op jit(solution)/shard_map/early/pallas_call | solution.py:212
  6.6 0.0 collective-permute-done.earlier
  6.6 0.5 conv.1
  7.1 1.3 %collective-permute-start.1 = (bf16[128,256]{1,0:T(8,128)(2,1)S(1)}, bf16[128,256]{1,0:T(8,128)(2,1)S(1)}, u32[]{:S(2)}, u32[]{:S(2)}) collective-permute-start(bf16[128,256]{1,0:T(8,128)(2,1)S(1)} %get-tuple-element.26), channel_id=1, source_target_pairs={{0,1},{1,2},{2,3},{3,0},{4,5},{5,6},{6,7},{7,4},{8,9},{9,10},{10,1... | collective-permute-start | bytes 196616 | tf_op jit(solution)/shard_map/ppermute | solution.py:243
  8.4 2.5 %collective-permute-start.2 = (bf16[128,256]{1,0:T(8,128)(2,1)S(1)}, bf16[128,256]{1,0:T(8,128)(2,1)S(1)}, u32[]{:S(2)}, u32[]{:S(2)}) collective-permute-start(bf16[128,256]{1,0:T(8,128)(2,1)S(1)} %get-tuple-element.27), channel_id=1, source_target_pairs={{0,2},{1,3},{2,0},{3,1},{4,6},{5,7},{6,4},{7,5},{8,10},{9,11},{10,... | collective-permute-start | bytes 196616 | tf_op jit(solution)/shard_map/ppermute | solution.py:243
  10.9 1.1 %collective-permute-start.3 = (bf16[128,256]{1,0:T(8,128)(2,1)S(1)}, bf16[128,256]{1,0:T(8,128)(2,1)S(1)}, u32[]{:S(2)}, u32[]{:S(2)}) collective-permute-start(bf16[128,256]{1,0:T(8,128)(2,1)S(1)} %get-tuple-element.28), channel_id=1, source_target_pairs={{0,3},{1,0},{2,1},{3,2},{4,7},{5,4},{6,5},{7,6},{8,11},{9,8},{10,9... | collective-permute-start | bytes 196616 | tf_op jit(solution)/shard_map/ppermute | solution.py:243
  12.0 2.4 %slots.1 = (s32[2,128]{1,0:T(2,128)S(1)}, bf16[1024,2048]{1,0:T(8,128)(2,1)S(1)}, bf16[128,2048]{1,0:T(8,128)(2,1)S(1)}, f32[1,2048]{1,0:T(1,128)S(1)}) custom-call(s32[2,128]{1,0:T(2,128)} %bitcast.22, bf16[1024,2048]{1,0:T(8,128)(2,1)} %proj.1, bf16[128,2048]{1,0:T(8,128)(2,1)} %residual.1, f32[1,2048]{1,0:T(1,128)} %bitcast.19), custom_call_target="tpu_custom_call" | custom-call | flops 1073741824 | bytes 8388608 | tf_op jit(solution)/shard_map/slots/pallas_call | solution.py:247
  14.4 0.0 collective-permute-done.1.r1
  14.4 0.0 collective-permute-done.2.r2
  14.4 0.0 collective-permute-done.3.r3
  14.4 0.0 copy-start
  14.5 0.0 copy-start.1
  14.5 1.7 %mix.1 = (bf16[1024,1024]{1,0:T(8,128)(2,1)S(1)}, f32[128,2048]{1,0:T(8,128)S(1)}) custom-call(s32[1]{0:T(128)} %bitcast.place, bf16[128,256]{1,0:T(8,128)(2,1)S(1)} %get-tuple-element.25.r0, bf16[128,256]{1,0:T(8,128)(2,1)S(1)} %collective-permute-done.1.r1, bf16[128,256]{1,0:T(8,128)(2,1)S(1)} %collective-permute-done.2.r2, ...), custom_call_target="tpu_custom_call" | custom-call | flops 1073741824 | bytes 8388608 | tf_op jit(solution)/shard_map/mix/pallas_call | solution.py:256
  16.1 42.1 %all_to_all.10 = bf16[128,8,1024]{2,1,0:T(8,128)(2,1)S(1)} all-to-all(bf16[128,8,1024]{2,1,0:T(8,128)(2,1)S(1)} %bitcast.12), channel_id=1, replica_groups=mesh['sp'=32,'tp'=4] {'sp','tp'}, dimensions={0} | all-to-all | bytes 4194304 | tf_op jit(solution)/shard_map/all_to_all | solution.py:262
  58.2 0.0 copy-done
  58.2 0.0 copy-done.1
  58.2 8.7 %experts.1 = bf16[1024,1024]{1,0:T(8,128)(2,1)S(1)} custom-call(bf16[1024,1024]{1,0:T(8,128)(2,1)S(1)} %bitcast.14, bf16[2048,1024]{1,0:T(8,128)(2,1)S(1)} %bitcast.16, bf16[2048,1024]{1,0:T(8,128)(2,1)S(1)} %bitcast.17, bf16[1024,2048]{1,0:T(8,128)(2,1)} %bitcast.23), custom_call_target="tpu_custom_call" | custom-call | flops 6442450944 | bytes 16777216 | tf_op jit(solution)/shard_map/experts/pallas_call | solution.py:264
  67.0 0.0 copy-start.2
  67.0 34.2 %all_to_all.11 = bf16[128,8,1024]{2,1,0:T(8,128)(2,1)S(1)} all-to-all(bf16[128,8,1024]{2,1,0:T(8,128)(2,1)S(1)} %bitcast.15), channel_id=1, replica_groups=mesh['sp'=32,'tp'=4] {'sp','tp'}, dimensions={0} | all-to-all | bytes 4194304 | tf_op jit(solution)/shard_map/all_to_all | solution.py:274
  101.1 0.0 copy-done.2
  101.1 2.3 %combine.1 = bf16[128,2048]{1,0:T(8,128)(2,1)} custom-call(bf16[1024,1024]{1,0:T(8,128)(2,1)S(1)} %bitcast.13, f32[128,2048]{1,0:T(8,128)S(1)} %get-tuple-element.34.carried, s32[2,128]{1,0:T(2,128)S(1)} %get-tuple-element.32.tgt, f32[2,128]{1,0:T(2,128)S(1)} %bitcast.18), custom_call_target="tpu_custom_call" | custom-call | flops 1073741824 | bytes 4194304 | tf_op jit(solution)/shard_map/combine/pallas_call | solution.py:275
Async XLA Ops:
  0.9 5.8 %collective-permute-start = (f32[4,256]{1,0:T(4,128)S(1)}, f32[4,256]{1,0:T(4,128)S(1)}, u32[]{:S(2)}, u32[]{:S(2)}) collective-permute-start(f32[4,256]{1,0:T(4,128)S(1)} %edge.1), channel_id=1, source_target_pairs={{0,4},{4,8},{8,12},{12,16},{16,20},{20,24},{24,28},{28,32},{32,36}... | collective-permute-start | bytes 12296 | tf_op jit(solution)/shard_map/ppermute | solution.py:234
  7.1 7.3 %collective-permute-start.1 = (bf16[128,256]{1,0:T(8,128)(2,1)S(1)}, bf16[128,256]{1,0:T(8,128)(2,1)S(1)}, u32[]{:S(2)}, u32[]{:S(2)}) collective-permute-start(bf16[128,256]{1,0:T(8,128)(2,1)S(1)} %get-tuple-element.26), channel_id=1, source_target_pairs={{0,1},{1,2},{2,3},{3,0},{4,5},{5,6},{6,7},{7,4},{8,9},{9,10},{10,1... | collective-permute-start | bytes 196616 | tf_op jit(solution)/shard_map/ppermute | solution.py:243
  8.4 6.0 %collective-permute-start.2 = (bf16[128,256]{1,0:T(8,128)(2,1)S(1)}, bf16[128,256]{1,0:T(8,128)(2,1)S(1)}, u32[]{:S(2)}, u32[]{:S(2)}) collective-permute-start(bf16[128,256]{1,0:T(8,128)(2,1)S(1)} %get-tuple-element.27), channel_id=1, source_target_pairs={{0,2},{1,3},{2,0},{3,1},{4,6},{5,7},{6,4},{7,5},{8,10},{9,11},{10,... | collective-permute-start | bytes 196616 | tf_op jit(solution)/shard_map/ppermute | solution.py:243
  10.9 3.5 %collective-permute-start.3 = (bf16[128,256]{1,0:T(8,128)(2,1)S(1)}, bf16[128,256]{1,0:T(8,128)(2,1)S(1)}, u32[]{:S(2)}, u32[]{:S(2)}) collective-permute-start(bf16[128,256]{1,0:T(8,128)(2,1)S(1)} %get-tuple-element.28), channel_id=1, source_target_pairs={{0,3},{1,0},{2,1},{3,2},{4,7},{5,4},{6,5},{7,6},{8,11},{9,8},{10,9... | collective-permute-start | bytes 196616 | tf_op jit(solution)/shard_map/ppermute | solution.py:243
  14.4 43.8 %copy-start = (bf16[1,2048,1024]{2,1,0:T(8,128)(2,1)S(1)}, bf16[1,2048,1024]{2,1,0:T(8,128)(2,1)}, u32[]{:S(2)}) copy-start(bf16[1,2048,1024]{2,1,0:T(8,128)(2,1)} %param.23) | copy-start | bytes 12582916
  14.5 43.8 %copy-start.1 = (bf16[1,2048,1024]{2,1,0:T(8,128)(2,1)S(1)}, bf16[1,2048,1024]{2,1,0:T(8,128)(2,1)}, u32[]{:S(2)}) copy-start(bf16[1,2048,1024]{2,1,0:T(8,128)(2,1)} %param.24) | copy-start | bytes 12582916
  67.0 34.2 %copy-start.2 = (f32[128,2]{0,1:T(2,128)S(1)}, f32[128,2]{0,1:T(2,128)}, u32[]{:S(2)}) copy-start(f32[128,2]{0,1:T(2,128)} %param.22) | copy-start | bytes 3076

commit v3 on v2

v3 whole, which is shorter than its diff:
```python
import functools
import jax
import jax.numpy as jnp
from jax import lax
from jax.experimental import pallas as pl
from jax.experimental.pallas import tpu as pltpu
from jax.sharding import PartitionSpec as P

F32 = jnp.float32
BF16 = jnp.bfloat16
EARLY = 62
SLOTS = 56
ORDER = (2, 1, 3)
VM = pl.BlockSpec(memory_space=pltpu.VMEM)
SM = pl.BlockSpec(memory_space=pltpu.SMEM)
HB = pl.BlockSpec(memory_space=pl.ANY)


def dot(a, b):
    return jnp.dot(a, b, preferred_element_type=F32)


def edge_kernel(x, g_in, docs, out, xv, gv, dv, sem):
    rows = x.shape[0]
    copies = [
        pltpu.make_async_copy(x.at[rows - 16 :, :], xv, sem.at[0]),
        pltpu.make_async_copy(g_in.at[rows - 16 :, :], gv, sem.at[1]),
        pltpu.make_async_copy(docs, dv, sem.at[2]),
    ]
    for copy in copies:
        copy.start()
    for copy in copies:
        copy.wait()
    prod = xv[...].astype(F32) * gv[...].astype(F32)
    last = dv.shape[0] - 1
    ids = jnp.broadcast_to(dv[last : last + 1, :].astype(F32), (128, 128)).T
    out[0:2, :] = prod[14:16, :]
    for c in range(out.shape[1] // 128):
        out[2:4, 128 * c : 128 * c + 128] = ids[126:128, :]


def taps_of(taps):
    return [taps[k : k + 1, :].astype(F32) for k in range(3)]


def conv_rows(window, ids, g_out, taps):
    count = window.shape[0] - 8
    cur = ids[8:]
    parts = []
    for half in range(window.shape[1] // 128):
        c = slice(128 * half, 128 * half + 128)
        back1 = jnp.where(ids[7:-1] == cur, window[7:-1, c], 0.0)
        back2 = jnp.where(ids[6:-2] == cur, window[6:-2, c], 0.0)
        mixed = taps[2][:, c] * window[8:, c] + taps[1][:, c] * back1 + taps[0][:, c] * back2
        parts.append((g_out[:, c].astype(F32) * mixed).astype(BF16))
    return parts


def slots_kernel(ids, proj, residual, gain, onehot, pick, proj_v, residual_v, gain_v, iv, sem):
    tokens = ids.shape[1]
    depth = proj.shape[0] // 4
    moves = [(ids, iv), (residual, residual_v), (gain, gain_v)]
    moves += [(proj.at[depth * j : depth * j + depth, :], proj_v.at[depth * j : depth * j + depth, :]) for j in range(4)]
    copies = [pltpu.make_async_copy(s, d, sem.at[i]) for i, (s, d) in enumerate(moves)]
    for copy in copies:
        copy.start()
    copies[0].wait()
    first = iv[0:1, :]
    second = iv[1:2, :]
    expert = lax.broadcasted_iota(jnp.int32, (128, tokens), 0)
    m0 = (expert == first).astype(F32)
    m1 = (expert == second).astype(F32)
    r = lax.broadcasted_iota(jnp.int32, (tokens, tokens), 0)
    c = lax.broadcasted_iota(jnp.int32, (tokens, tokens), 1)
    before = (r < c).astype(F32).astype(BF16)
    n0 = dot(m0.astype(BF16), before)
    n1 = dot(m1.astype(BF16), before) + jnp.sum(m0, axis=1, keepdims=True)
    rank0 = jnp.sum(m0 * n0, axis=0, keepdims=True).astype(jnp.int32)
    rank1 = jnp.sum(m1 * n1, axis=0, keepdims=True).astype(jnp.int32)
    target = [first * 8 + rank0, second * 8 + rank1]
    slots = onehot.shape[0]
    row = lax.broadcasted_iota(jnp.int32, (slots, tokens), 0)
    onehot[:, 0:tokens] = ((row == target[0]) | (row == target[1])).astype(F32).astype(BF16)
    onehot[:, tokens:] = ((row == target[0] + 4) | (row == target[1] + 4)).astype(F32).astype(BF16)
    for k in range(2):
        line = jnp.broadcast_to(target[k].astype(F32), (128, tokens)).T
        for n in range(slots // 128):
            lane = (lax.broadcasted_iota(jnp.int32, (tokens, 128), 1) + 128 * n).astype(F32)
            span = slice(128 * n, 128 * n + 128)
            pick[0, k * tokens : (k + 1) * tokens, span] = (line == lane).astype(F32).astype(BF16)
            pick[1, k * tokens : (k + 1) * tokens, span] = (line + 4.0 == lane).astype(F32).astype(BF16)
    for copy in copies[1:]:
        copy.wait()


def early_kernel(place, x, g_in, g_out, taps, docs, o0, o1, o2, o3, head, head_ids, gate_v, taps_v,
                 xv, gv, ov, dv, prod, doc_col, sem):
    rows = x.shape[0]
    part = o0.shape[0]
    moves = [(docs, dv), (taps, taps_v), (x, xv), (g_in, gv), (g_out, ov)]
    copies = [pltpu.make_async_copy(s, d, sem.at[i]) for i, (s, d) in enumerate(moves)]
    for copy in copies:
        copy.start()
    for copy in copies:
        copy.wait()
    prod[0:8, :] = jnp.zeros((8, x.shape[1]), F32)
    prod[8:, :] = xv[...].astype(F32) * gv[...].astype(F32)
    doc_col[0:8, :] = jnp.zeros((8, 128), F32)
    for block in range(rows // 128):
        line = jnp.broadcast_to(dv[block : block + 1, :].astype(F32), (128, 128))
        doc_col[8 + 128 * block : 136 + 128 * block, :] = line.T
    head[...] = prod[8:24, :]
    head_ids[...] = doc_col[8:24, :]
    gate_v[...] = ov[0:16, :]
    weights = taps_of(taps_v)
    here = place[0]
    for shift, out in enumerate((o0, o1, o2, o3)):
        start = pl.multiple_of(lax.rem(here + shift, 4) * part, part)
        pieces = conv_rows(
            prod[pl.ds(start, part + 8), :], doc_col[pl.ds(start, part + 8), :],
            ov[pl.ds(start, part), :], weights,
        )
        for half, piece in enumerate(pieces):
            out[:, 128 * half : 128 * half + 128] = piece


def fix_kernel(place, earlier, head, head_ids, g_out, taps, i0, i1, i2, i3, o0, o1, o2, o3):
    width = head.shape[1]
    here = place[0]
    window = jnp.concatenate([jnp.zeros((6, width), F32), earlier[0:2, :], head[...]], axis=0)
    ids = jnp.concatenate([jnp.zeros((6, 128), F32), earlier[2:4, 0:128], head_ids[...]], axis=0)
    pieces = conv_rows(window, ids, g_out[...], taps_of(taps))
    for shift, out in enumerate((o0, o1, o2, o3)):

        @pl.when(lax.rem(here + shift, 4) == 0)
        def _():
            for half, piece in enumerate(pieces):
                out[0:16, 128 * half : 128 * half + 128] = piece


def mix_kernel(place, r0, r1, r2, r3, residual, proj, gain, onehot, buf, carried, halves):
    here = place[0]
    width = residual.shape[1]
    half = width // 2
    tokens = residual.shape[0]
    step = 512
    total = jnp.zeros((tokens, 1), F32)
    for n in range(width // step):
        c = slice(n * step, n * step + step)
        acc = None
        for shift, part in enumerate((r0, r1, r2, r3)):
            depth = part.shape[1]
            start = pl.multiple_of(lax.rem(here + 4 - shift, 4) * depth, depth)
            term = dot(part[...], proj[pl.ds(start, depth), c])
            acc = term if acc is None else acc + term
        value = residual[:, c].astype(F32) + acc.astype(BF16).astype(F32)
        carried[:, c] = value
        total = total + jnp.sum(value * value, axis=1, keepdims=True)
    scale = lax.rsqrt(total * (1.0 / width) + 1e-06)
    for n in range(width // step):
        c = slice(n * step, n * step + step)
        value = (carried[:, c] * scale * gain[:, c]).astype(BF16)
        h = (n * step) // half
        halves[h * tokens : (h + 1) * tokens, n * step - h * half : n * step - h * half + step] = value
    for n in range(half // 256):
        c = slice(n * 256, n * 256 + 256)
        buf[:, c] = dot(onehot[...], halves[:, c]).astype(BF16)


def expert_kernel(arrived, wg, wu, wd, out, xv, hv):
    rows, half = arrived.shape
    blocks = wg.shape[1] // 256
    cols = [slice(256 * j, 256 * j + 256) for j in range(blocks)]
    low = lax.broadcasted_iota(jnp.int32, (rows // 16, 8, 256), 1) < 4
    for j, c in enumerate(cols):
        value = arrived[:, c].astype(F32).reshape(rows // 16, 2, 8, 256)
        even, odd = value[:, 0], value[:, 1]
        lo = jnp.where(low, even, pltpu.roll(odd, 4, 1))
        hi = jnp.where(low, pltpu.roll(even, 4, 1), odd)
        xv[:, c] = lo.reshape(rows // 2, 256).astype(BF16)
        xv[:, half + 256 * j : half + 256 * j + 256] = hi.reshape(rows // 2, 256).astype(BF16)
    for j, c in enumerate(cols):
        gate = dot(xv[...], wg[:, c])
        up = dot(xv[...], wu[:, c])
        hv[:, c] = (gate / (1.0 + jnp.exp(-gate)) * up).astype(BF16)
    for j, c in enumerate(cols):
        lo = dot(hv[...], wd[:, c]).reshape(rows // 16, 8, 256)
        hi = dot(hv[...], wd[:, half + 256 * j : half + 256 * j + 256]).reshape(rows // 16, 8, 256)
        even = jnp.where(low, lo, pltpu.roll(hi, 4, 1))
        odd = jnp.where(low, pltpu.roll(lo, 4, 1), hi)
        out[:, c] = jnp.stack([even, odd], axis=1).reshape(rows, 256).astype(BF16)


def combine_kernel(returned, carried, pick, weights, out, ov, sem):
    tokens = carried.shape[0]
    rows, half = returned.shape
    w = [jnp.broadcast_to(weights[k : k + 1, :], (128, tokens)).T[:, 0:1] for k in range(2)]
    copies = []
    for h in range(2):
        for n in range(half // 256):
            c = slice(256 * n, 256 * n + 256)
            d = slice(h * half + 256 * n, h * half + 256 * n + 256)
            both = dot(pick[h], returned[:, c])
            ov[:, d] = (carried[:, d] + (w[0] * both[:tokens] + w[1] * both[tokens:])).astype(BF16)
            copy = pltpu.make_async_copy(ov.at[:, d], out.at[:, d], sem.at[len(copies)])
            copy.start()
            copies.append(copy)
    for copy in copies:
        copy.wait()


def call(kernel, out_shape, in_specs, out_specs, scratch, vmem_mib, flops=0, nbytes=0, alias={}, name=None):
    return pl.pallas_call(
        kernel,
        out_shape=out_shape,
        in_specs=in_specs,
        out_specs=out_specs,
        scratch_shapes=scratch,
        input_output_aliases=alias,
        name=name,
        compiler_params=pltpu.CompilerParams(vmem_limit_bytes=int(vmem_mib * 1048576)),
        cost_estimate=pl.CostEstimate(flops=flops, bytes_accessed=nbytes, transcendentals=0),
    )


def shape(dims, kind):
    return jax.ShapeDtypeStruct(dims, kind)


def on_device(conv_input, gate_inner, gate_outer, conv_taps, doc_ids, residual_in, out_proj,
              norm_gain, expert_ids, expert_weights, gate_proj, up_proj, down_proj):
    length, channels = conv_input.shape
    tokens, width = residual_in.shape
    sp_count = lax.axis_size("sp")
    tp_count = lax.axis_size("tp")
    experts = sp_count * tp_count
    place = lax.axis_index("tp").reshape(1)
    docs = doc_ids.reshape(-1, 128)
    edge = call(
        edge_kernel, pltpu.VMEM((4, channels), F32), [HB] * 3, VM,
        [pltpu.VMEM((16, channels), BF16), pltpu.VMEM((16, channels), BF16),
         pltpu.VMEM(docs.shape, jnp.int32), pltpu.SemaphoreType.DMA((3,))],
        63, 1 << 20, 1 << 16, name="edge",
    )(conv_input, gate_inner, docs)
    earlier = lax.ppermute(edge, "sp", [(i, i + 1) for i in range(sp_count - 1)])
    gain = norm_gain.reshape(1, -1)
    rows = experts * 8
    half = width // 2
    piece = pltpu.VMEM((tokens, channels), BF16)
    outs = (piece,) * 4 + (
        pltpu.VMEM((16, channels), F32), pltpu.VMEM((16, 128), F32), pltpu.VMEM((16, channels), BF16),
        pltpu.VMEM(conv_taps.shape, BF16),
    )
    *raw, head, head_ids, gate_v, taps_v = call(
        early_kernel, outs, [SM] + [HB] * 5, (VM,) * len(outs),
        [
            pltpu.VMEM((length, channels), BF16), pltpu.VMEM((length, channels), BF16),
            pltpu.VMEM((length, channels), BF16), pltpu.VMEM(docs.shape, jnp.int32),
            pltpu.VMEM((length + 8, channels), F32),
            pltpu.VMEM((length + 8, 128), F32), pltpu.SemaphoreType.DMA((5,)),
        ],
        EARLY, 1 << 28, 1 << 20, name="early",
    )(place, conv_input, gate_inner, gate_outer, conv_taps, docs)
    sent = call(
        fix_kernel, (piece,) * 4, [SM] + [VM] * 9, (VM,) * 4, [], 4, 1 << 20, 1 << 18,
        alias={6 + k: k for k in range(4)}, name="fix",
    )(place, earlier, head, head_ids, gate_v, taps_v, *raw)
    parts = [sent[0], None, None, None]
    for d in ORDER:
        parts[d] = lax.ppermute(sent[d], "tp", [(i, (i + d) % tp_count) for i in range(tp_count)])
    held = (
        pltpu.VMEM((rows, 2 * tokens), BF16), pltpu.VMEM((2, 2 * tokens, rows), BF16),
        pltpu.VMEM(out_proj.shape, BF16), pltpu.VMEM(residual_in.shape, BF16), pltpu.VMEM(gain.shape, F32),
    )
    onehot, pick, proj_v, residual_v, gain_v = call(
        slots_kernel, held, [HB] * 4, (VM,) * 5,
        [pltpu.VMEM((2, tokens), jnp.int32), pltpu.SemaphoreType.DMA((7,))],
        SLOTS, 1 << 30, 1 << 23, name="slots",
    )(expert_ids.T, out_proj, residual_in, gain)
    buf, carried = call(
        mix_kernel, (shape((rows, half), BF16), shape((tokens, width), F32)),
        [SM] + [VM] * 8, (VM, VM),
        [pltpu.VMEM((2 * tokens, half), BF16)],
        12, 8 << 30, 1 << 23, name="mix",
    )(place, *parts, residual_v, proj_v, gain_v, onehot)
    arrived = lax.all_to_all(buf.reshape(experts, 8, half), ("sp", "tp"), split_axis=0, concat_axis=0, tiled=True)
    hidden = gate_proj.shape[2]
    result = call(
        expert_kernel, shape((rows, half), BF16), [VM] * 4, VM,
        [
            pltpu.VMEM((rows // 2, width), BF16),
            pltpu.VMEM((rows // 2, hidden), BF16),
        ],
        20, 6 << 30, 1 << 24, name="experts",
    )(arrived.reshape(rows, half), gate_proj[0], up_proj[0], down_proj[0])
    returned = lax.all_to_all(result.reshape(experts, 8, half), ("sp", "tp"), split_axis=0, concat_axis=0, tiled=True)
    return call(
        combine_kernel, shape((tokens, width), BF16), [VM] * 4, HB,
        [pltpu.VMEM((tokens, width), BF16), pltpu.SemaphoreType.DMA((8,))],
        12, 1 << 30, 1 << 22, name="combine",
    )(returned.reshape(rows, half), carried, pick, expert_weights.T)


def solution(mesh):
    both = ("sp", "tp")
    in_specs = (
        P("sp", "tp"),
        P("sp", "tp"),
        P("sp", "tp"),
        P(None, "tp"),
        P("sp"),
        P(both, None),
        P(),
        P(),
        P(both, None),
        P(both, None),
        P(both, None, None),
        P(both, None, None),
        P(both, None, None),
    )
    return jax.shard_map(
        on_device, mesh=mesh, in_specs=in_specs, out_specs=P(both, None), check_vma=False
    )
```

time: 104 us -> 101 us (0.971)
  Pallas kernels: 17.6 us -> 15.4 us
    pallas_call x5, Pallas kernels: 15 us -> 12.9 us  [the longest x1 6.69 us: on_device(): call(expert_kernel, shape((rows, half), BF16), [VM] * 4, VM, [pltpu.VMEM(...]
  transfers between devices with their start and end apart: 4 -> 4, of which waited for: 0 -> 0; matrix products, arithmetic and copies ran while one was open for 0% -> 0% of each run, Pallas kernels for 3% -> 4%
where the time goes in v3:
time: 101 us
  blocking collectives  75.6 us (75%)
  Pallas kernels  15.4 us (15%)
  starting transfers between devices  9.47 us (9%)
    all_to_all x1, blocking collectives, on_device(): lax.all_to_all(buf.reshape(experts, 8, half), ('sp', 'tp'), split_axis=0,...  41.4 us
    all_to_all x1, blocking collectives, on_device(): lax.all_to_all(result.reshape(experts, 8, half), ('sp', 'tp'), split_axis...  34.2 us
    pallas_call x1, Pallas kernels, on_device(): call(expert_kernel, shape((rows, half), BF16), [VM] * 4, VM, [pltpu.VMEM(...  6.69 us
    ppermute x3, starting transfers between devices, on_device(): lax.ppermute(sent[d], 'tp', [(i, (i + d) % tp_count) for i in range(tp_co...  4.89 us
    ppermute x1, starting transfers between devices, on_device(): lax.ppermute(edge, 'sp', [(i, i + 1) for i in range(sp_count - 1)])  4.58 us
    pallas_call x1, Pallas kernels, on_device(): call(slots_kernel, held, [HB] * 4, (VM,) * 5, [pltpu.VMEM((2, tokens), jn...  2.42 us
    pallas_call x1, Pallas kernels, on_device(): call(combine_kernel, shape((tokens, width), BF16), [VM] * 4, HB, [pltpu.V...  2.04 us
  transfers between devices with their start and end apart: 4, of which 0 were waited for; matrix products, arithmetic and copies ran while one was open for 0% of the time, Pallas kernels for 4%

profile of v3, /device:TPU:1, one launch (start us, length us, event | category | flops | bytes accessed | tf_op | source)
XLA Modules:
  0.0 100.6 jit_solution(209087079680546386)
XLA Ops:
  0.0 0.8 edge.1
  0.9 4.6 %collective-permute-start = (f32[4,256]{1,0:T(4,128)S(1)}, f32[4,256]{1,0:T(4,128)S(1)}, u32[]{:S(2)}, u32[]{:S(2)}) collective-permute-start(f32[4,256]{1,0:T(4,128)S(1)} %edge.1), channel_id=1, source_target_pairs={{0,4},{4,8},{8,12},{12,16},{16,20},{20,24},{24,28},{28,32},{32,36}... | collective-permute-start | bytes 12296 | tf_op jit(solution)/shard_map/ppermute | solution.py:245
  5.4 1.7 %early.1 = (bf16[128,256]{1,0:T(8,128)(2,1)S(1)}, bf16[128,256]{1,0:T(8,128)(2,1)S(1)}, bf16[128,256]{1,0:T(8,128)(2,1)S(1)}, bf16[128,256]{1,0:T(8,128)(2,1)S(1...) custom-call(s32[1]{0:T(128)} %bitcast.place, ...), custom_call_target="tpu_custom_call" | custom-call | flops 268435456 | bytes 1048576 | tf_op jit(solution)/shard_map/early/pallas_call | solution.py:254
  7.2 0.0 collective-permute-done.earlier
  7.2 1.3 %collective-permute-start.1 = (bf16[128,256]{1,0:T(8,128)(2,1)S(1)}, bf16[128,256]{1,0:T(8,128)(2,1)S(1)}, u32[]{:S(2)}, u32[]{:S(2)}) collective-permute-start(bf16[128,256]{1,0:T(8,128)(2,1)S(1)} %get-tuple-element.33), channel_id=1, source_target_pairs={{0,1},{1,2},{2,3},{3,0},{4,5},{5,6},{6,7},{7,4},{8,9},{9,10},{10,1... | collective-permute-start | bytes 196616 | tf_op jit(solution)/shard_map/ppermute | solution.py:270
  8.5 2.5 %collective-permute-start.2 = (bf16[128,256]{1,0:T(8,128)(2,1)S(1)}, bf16[128,256]{1,0:T(8,128)(2,1)S(1)}, u32[]{:S(2)}, u32[]{:S(2)}) collective-permute-start(bf16[128,256]{1,0:T(8,128)(2,1)S(1)} %get-tuple-element.34), channel_id=1, source_target_pairs={{0,2},{1,3},{2,0},{3,1},{4,6},{5,7},{6,4},{7,5},{8,10},{9,11},{10,... | collective-permute-start | bytes 196616 | tf_op jit(solution)/shard_map/ppermute | solution.py:270
  11.0 1.1 %collective-permute-start.3 = (bf16[128,256]{1,0:T(8,128)(2,1)S(1)}, bf16[128,256]{1,0:T(8,128)(2,1)S(1)}, u32[]{:S(2)}, u32[]{:S(2)}) collective-permute-start(bf16[128,256]{1,0:T(8,128)(2,1)S(1)} %get-tuple-element.35), channel_id=1, source_target_pairs={{0,3},{1,0},{2,1},{3,2},{4,7},{5,4},{6,5},{7,6},{8,11},{9,8},{10,9... | collective-permute-start | bytes 196616 | tf_op jit(solution)/shard_map/ppermute | solution.py:270
  12.1 2.4 %slots.1 = (bf16[1024,256]{1,0:T(8,128)(2,1)S(1)}, bf16[2,256,1024]{2,1,0:T(8,128)(2,1)S(1)}, bf16[1024,2048]{1,0:T(8,128)(2,1)S(1)}, bf16[128,2048]{1,0:T(8,128)(2,1)S(1)}, f32[1,2048]{1,0:T(1,128)S(1)}) custom-call(s32[2,128]{1,0:T(2,128)} %bitcast.23, bf16[1024,2048]{1,0:T(8,128)(2,1)} %proj.1, bf16[128,2048]{1,0:T(8,128)(2,1)} %residual.1, ...), custom_call_target="tpu_custom_call" | custom-call | flops 1073741824 | bytes 8388608 | tf_op jit(solution)/shard_map/slots/pallas_call | solution.py:275
  14.5 0.0 collective-permute-done.1.r1
  14.6 0.0 collective-permute-done.2.r2
  14.6 0.0 collective-permute-done.3.r3
  14.6 0.0 copy-start.2
  14.6 0.0 copy-start.3
  14.6 1.6 %mix.1 = (bf16[1024,1024]{1,0:T(8,128)(2,1)S(1)}, f32[128,2048]{1,0:T(8,128)S(1)}) custom-call(s32[1]{0:T(128)} %bitcast.place, bf16[128,256]{1,0:T(8,128)(2,1)S(1)} %get-tuple-element.32.r0, bf16[128,256]{1,0:T(8,128)(2,1)S(1)} %collective-permute-done.1.r1, bf16[128,256]{1,0:T(8,128)(2,1)S(1)} %collective-permute-done.2.r2, ...), custom_call_target="tpu_custom_call" | custom-call | flops 8589934592 | bytes 8388608 | tf_op jit(solution)/shard_map/mix/pallas_call | solution.py:280
  16.2 0.0 copy-start.1
  16.2 41.4 %all_to_all.10 = bf16[128,8,1024]{2,1,0:T(8,128)(2,1)S(1)} all-to-all(bf16[128,8,1024]{2,1,0:T(8,128)(2,1)S(1)} %bitcast.13), channel_id=1, replica_groups=mesh['sp'=32,'tp'=4] {'sp','tp'}, dimensions={0} | all-to-all | bytes 4194304 | tf_op jit(solution)/shard_map/all_to_all | solution.py:286
  57.7 0.0 copy-done.2
  57.7 0.0 copy-done.3
  57.7 0.0 copy-done.1
  57.7 6.7 %experts.1 = bf16[1024,1024]{1,0:T(8,128)(2,1)S(1)} custom-call(bf16[1024,1024]{1,0:T(8,128)(2,1)S(1)} %bitcast.14, bf16[2048,1024]{1,0:T(8,128)(2,1)S(1)} %bitcast.17, bf16[2048,1024]{1,0:T(8,128)(2,1)S(1)} %bitcast.18, bf16[1024,2048]{1,0:T(8,128)(2,1)S(1)} %bitcast.19), custom_call_target="tpu_custom_call" | custom-call | flops 6442450944 | bytes 16777216 | tf_op jit(solution)/shard_map/experts/pallas_call | solution.py:288
  64.4 0.0 copy-start
  64.4 34.2 %all_to_all.11 = bf16[128,8,1024]{2,1,0:T(8,128)(2,1)S(1)} all-to-all(bf16[128,8,1024]{2,1,0:T(8,128)(2,1)S(1)} %bitcast.15), channel_id=1, replica_groups=mesh['sp'=32,'tp'=4] {'sp','tp'}, dimensions={0} | all-to-all | bytes 4194304 | tf_op jit(solution)/shard_map/all_to_all | solution.py:296
  98.6 0.0 copy-done
  98.6 2.0 %combine.1 = bf16[128,2048]{1,0:T(8,128)(2,1)} custom-call(bf16[1024,1024]{1,0:T(8,128)(2,1)S(1)} %bitcast.12, f32[128,2048]{1,0:T(8,128)S(1)} %get-tuple-element.41.carried, bf16[2,256,1024]{2,1,0:T(8,128)(2,1)S(1)} %get-tuple-element.42.pick, f32[2,128]{1,0:T(2,128)S(1)} %bitcast.16), custom_call_target="tpu_custom_call" | custom-call | flops 1073741824 | bytes 4194304 | tf_op jit(solution)/shard_map/combine/pallas_call | solution.py:297
  (1 shorter events, 0.0 us)
Async XLA Ops:
  0.9 6.3 %collective-permute-start = (f32[4,256]{1,0:T(4,128)S(1)}, f32[4,256]{1,0:T(4,128)S(1)}, u32[]{:S(2)}, u32[]{:S(2)}) collective-permute-start(f32[4,256]{1,0:T(4,128)S(1)} %edge.1), channel_id=1, source_target_pairs={{0,4},{4,8},{8,12},{12,16},{16,20},{20,24},{24,28},{28,32},{32,36}... | collective-permute-start | bytes 12296 | tf_op jit(solution)/shard_map/ppermute | solution.py:245
  7.2 7.3 %collective-permute-start.1 = (bf16[128,256]{1,0:T(8,128)(2,1)S(1)}, bf16[128,256]{1,0:T(8,128)(2,1)S(1)}, u32[]{:S(2)}, u32[]{:S(2)}) collective-permute-start(bf16[128,256]{1,0:T(8,128)(2,1)S(1)} %get-tuple-element.33), channel_id=1, source_target_pairs={{0,1},{1,2},{2,3},{3,0},{4,5},{5,6},{6,7},{7,4},{8,9},{9,10},{10,1... | collective-permute-start | bytes 196616 | tf_op jit(solution)/shard_map/ppermute | solution.py:270
  8.5 6.1 %collective-permute-start.2 = (bf16[128,256]{1,0:T(8,128)(2,1)S(1)}, bf16[128,256]{1,0:T(8,128)(2,1)S(1)}, u32[]{:S(2)}, u32[]{:S(2)}) collective-permute-start(bf16[128,256]{1,0:T(8,128)(2,1)S(1)} %get-tuple-element.34), channel_id=1, source_target_pairs={{0,2},{1,3},{2,0},{3,1},{4,6},{5,7},{6,4},{7,5},{8,10},{9,11},{10,... | collective-permute-start | bytes 196616 | tf_op jit(solution)/shard_map/ppermute | solution.py:270
  11.0 3.6 %collective-permute-start.3 = (bf16[128,256]{1,0:T(8,128)(2,1)S(1)}, bf16[128,256]{1,0:T(8,128)(2,1)S(1)}, u32[]{:S(2)}, u32[]{:S(2)}) collective-permute-start(bf16[128,256]{1,0:T(8,128)(2,1)S(1)} %get-tuple-element.35), channel_id=1, source_target_pairs={{0,3},{1,0},{2,1},{3,2},{4,7},{5,4},{6,5},{7,6},{8,11},{9,8},{10,9... | collective-permute-start | bytes 196616 | tf_op jit(solution)/shard_map/ppermute | solution.py:270
  14.6 43.1 %copy-start.2 = (bf16[1,2048,1024]{2,1,0:T(8,128)(2,1)S(1)}, bf16[1,2048,1024]{2,1,0:T(8,128)(2,1)}, u32[]{:S(2)}) copy-start(bf16[1,2048,1024]{2,1,0:T(8,128)(2,1)} %param.24) | copy-start | bytes 12582916
  14.6 43.1 %copy-start.3 = (bf16[1,1024,2048]{2,1,0:T(8,128)(2,1)S(1)}, bf16[1,1024,2048]{2,1,0:T(8,128)(2,1)}, u32[]{:S(2)}) copy-start(bf16[1,1024,2048]{2,1,0:T(8,128)(2,1)} %param.25) | copy-start | bytes 12582916
  16.2 41.5 %copy-start.1 = (bf16[1,2048,1024]{2,1,0:T(8,128)(2,1)S(1)}, bf16[1,2048,1024]{2,1,0:T(8,128)(2,1)}, u32[]{:S(2)}) copy-start(bf16[1,2048,1024]{2,1,0:T(8,128)(2,1)} %param.23) | copy-start | bytes 12582916
  64.4 34.2 %copy-start = (f32[128,2]{0,1:T(2,128)S(1)}, f32[128,2]{0,1:T(2,128)}, u32[]{:S(2)}) copy-start(f32[128,2]{0,1:T(2,128)} %param.22) | copy-start | bytes 3076

commit v4 on v3

--- a/solution.py
+++ b/solution.py
@@ -8,8 +8,12 @@
 
 F32 = jnp.float32
 BF16 = jnp.bfloat16
-EARLY = 62
-SLOTS = 56
+EDGE = 61
+EARLY = 24
+SLOTS = 8
+SLOT_FLOPS = 2 << 30
+EARLY_FLOPS = 8 << 30
+EDGE_FLOPS = 8 << 30
 ORDER = (2, 1, 3)
 VM = pl.BlockSpec(memory_space=pltpu.VMEM)
 SM = pl.BlockSpec(memory_space=pltpu.SMEM)
@@ -56,15 +60,8 @@
     return parts
 
 
-def slots_kernel(ids, proj, residual, gain, onehot, pick, proj_v, residual_v, gain_v, iv, sem):
-    tokens = ids.shape[1]
-    depth = proj.shape[0] // 4
-    moves = [(ids, iv), (residual, residual_v), (gain, gain_v)]
-    moves += [(proj.at[depth * j : depth * j + depth, :], proj_v.at[depth * j : depth * j + depth, :]) for j in range(4)]
-    copies = [pltpu.make_async_copy(s, d, sem.at[i]) for i, (s, d) in enumerate(moves)]
-    for copy in copies:
-        copy.start()
-    copies[0].wait()
+def slots_kernel(iv, onehot, pick):
+    tokens = iv.shape[1]
     first = iv[0:1, :]
     second = iv[1:2, :]
     expert = lax.broadcasted_iota(jnp.int32, (128, tokens), 0)
@@ -82,28 +79,19 @@
     row = lax.broadcasted_iota(jnp.int32, (slots, tokens), 0)
     onehot[:, 0:tokens] = ((row == target[0]) | (row == target[1])).astype(F32).astype(BF16)
     onehot[:, tokens:] = ((row == target[0] + 4) | (row == target[1] + 4)).astype(F32).astype(BF16)
-    for k in range(2):
-        line = jnp.broadcast_to(target[k].astype(F32), (128, tokens)).T
-        for n in range(slots // 128):
+    for k, (chosen, rank) in enumerate(((first, rank0), (second, rank1))):
+        line = jnp.broadcast_to((chosen * 4 + rank).astype(F32), (128, tokens)).T
+        for n in range(pick.shape[1] // 128):
             lane = (lax.broadcasted_iota(jnp.int32, (tokens, 128), 1) + 128 * n).astype(F32)
             span = slice(128 * n, 128 * n + 128)
-            pick[0, k * tokens : (k + 1) * tokens, span] = (line == lane).astype(F32).astype(BF16)
-            pick[1, k * tokens : (k + 1) * tokens, span] = (line + 4.0 == lane).astype(F32).astype(BF16)
-    for copy in copies[1:]:
-        copy.wait()
-
-
-def early_kernel(place, x, g_in, g_out, taps, docs, o0, o1, o2, o3, head, head_ids, gate_v, taps_v,
-                 xv, gv, ov, dv, prod, doc_col, sem):
-    rows = x.shape[0]
+            pick[k * tokens : (k + 1) * tokens, span] = (line == lane).astype(F32).astype(BF16)
+
+
+def early_kernel(place, xv, gv, ov, taps, dv, o0, o1, o2, o3, head, head_ids, gate_v, taps_v, prod, doc_col):
+    rows = xv.shape[0]
     part = o0.shape[0]
-    moves = [(docs, dv), (taps, taps_v), (x, xv), (g_in, gv), (g_out, ov)]
-    copies = [pltpu.make_async_copy(s, d, sem.at[i]) for i, (s, d) in enumerate(moves)]
-    for copy in copies:
-        copy.start()
-    for copy in copies:
-        copy.wait()
-    prod[0:8, :] = jnp.zeros((8, x.shape[1]), F32)
+    taps_v[...] = taps[...]
+    prod[0:8, :] = jnp.zeros((8, xv.shape[1]), F32)
     prod[8:, :] = xv[...].astype(F32) * gv[...].astype(F32)
     doc_col[0:8, :] = jnp.zeros((8, 128), F32)
     for block in range(rows // 128):
@@ -126,16 +114,17 @@
 
 def fix_kernel(place, earlier, head, head_ids, g_out, taps, i0, i1, i2, i3, o0, o1, o2, o3):
     width = head.shape[1]
+    part = i0.shape[0]
     here = place[0]
     window = jnp.concatenate([jnp.zeros((6, width), F32), earlier[0:2, :], head[...]], axis=0)
     ids = jnp.concatenate([jnp.zeros((6, 128), F32), earlier[2:4, 0:128], head_ids[...]], axis=0)
     pieces = conv_rows(window, ids, g_out[...], taps_of(taps))
-    for shift, out in enumerate((o0, o1, o2, o3)):
-
-        @pl.when(lax.rem(here + shift, 4) == 0)
-        def _():
-            for half, piece in enumerate(pieces):
-                out[0:16, 128 * half : 128 * half + 128] = piece
+    for shift, (old, out) in enumerate(zip((i0, i1, i2, i3), (o0, o1, o2, o3))):
+        out[16:part, :] = old[16:part, :]
+        mine = jnp.full((16, 128), lax.rem(here + shift, 4), jnp.int32) == 0
+        for half, piece in enumerate(pieces):
+            c = slice(128 * half, 128 * half + 128)
+            out[0:16, c] = jnp.where(mine, piece.astype(F32), old[0:16, c].astype(F32)).astype(BF16)
 
 
 def mix_kernel(place, r0, r1, r2, r3, residual, proj, gain, onehot, buf, carried, halves):
@@ -195,12 +184,17 @@
     tokens = carried.shape[0]
     rows, half = returned.shape
     w = [jnp.broadcast_to(weights[k : k + 1, :], (128, tokens)).T[:, 0:1] for k in range(2)]
+    low = lax.broadcasted_iota(jnp.int32, (rows // 16, 8, 256), 1) < 4
     copies = []
-    for h in range(2):
-        for n in range(half // 256):
-            c = slice(256 * n, 256 * n + 256)
+    for n in range(half // 256):
+        c = slice(256 * n, 256 * n + 256)
+        value = returned[:, c].astype(F32).reshape(rows // 16, 2, 8, 256)
+        even, odd = value[:, 0], value[:, 1]
+        lo = jnp.where(low, even, pltpu.roll(odd, 4, 1))
+        hi = jnp.where(low, pltpu.roll(even, 4, 1), odd)
+        for h, source in enumerate((lo, hi)):
             d = slice(h * half + 256 * n, h * half + 256 * n + 256)
-            both = dot(pick[h], returned[:, c])
+            both = dot(pick[...], source.reshape(rows // 2, 256).astype(BF16))
             ov[:, d] = (carried[:, d] + (w[0] * both[:tokens] + w[1] * both[tokens:])).astype(BF16)
             copy = pltpu.make_async_copy(ov.at[:, d], out.at[:, d], sem.at[len(copies)])
             copy.start()
@@ -209,14 +203,13 @@
         copy.wait()
 
 
-def call(kernel, out_shape, in_specs, out_specs, scratch, vmem_mib, flops=0, nbytes=0, alias={}, name=None):
+def call(kernel, out_shape, in_specs, out_specs, scratch, vmem_mib, flops=0, nbytes=0, name=None):
     return pl.pallas_call(
         kernel,
         out_shape=out_shape,
         in_specs=in_specs,
         out_specs=out_specs,
         scratch_shapes=scratch,
-        input_output_aliases=alias,
         name=name,
         compiler_params=pltpu.CompilerParams(vmem_limit_bytes=int(vmem_mib * 1048576)),
         cost_estimate=pl.CostEstimate(flops=flops, bytes_accessed=nbytes, transcendentals=0),
@@ -240,7 +233,7 @@
         edge_kernel, pltpu.VMEM((4, channels), F32), [HB] * 3, VM,
         [pltpu.VMEM((16, channels), BF16), pltpu.VMEM((16, channels), BF16),
          pltpu.VMEM(docs.shape, jnp.int32), pltpu.SemaphoreType.DMA((3,))],
-        63, 1 << 20, 1 << 16, name="edge",
+        EDGE, EDGE_FLOPS, 1 << 16, name="edge",
     )(conv_input, gate_inner, docs)
     earlier = lax.ppermute(edge, "sp", [(i, i + 1) for i in range(sp_count - 1)])
     gain = norm_gain.reshape(1, -1)
@@ -252,37 +245,27 @@
         pltpu.VMEM(conv_taps.shape, BF16),
     )
     *raw, head, head_ids, gate_v, taps_v = call(
-        early_kernel, outs, [SM] + [HB] * 5, (VM,) * len(outs),
-        [
-            pltpu.VMEM((length, channels), BF16), pltpu.VMEM((length, channels), BF16),
-            pltpu.VMEM((length, channels), BF16), pltpu.VMEM(docs.shape, jnp.int32),
-            pltpu.VMEM((length + 8, channels), F32),
-            pltpu.VMEM((length + 8, 128), F32), pltpu.SemaphoreType.DMA((5,)),
-        ],
-        EARLY, 1 << 28, 1 << 20, name="early",
+        early_kernel, outs, [SM] + [VM] * 5, (VM,) * len(outs),
+        [pltpu.VMEM((length + 8, channels), F32), pltpu.VMEM((length + 8, 128), F32)],
+        EARLY, EARLY_FLOPS, 1 << 20, name="early",
     )(place, conv_input, gate_inner, gate_outer, conv_taps, docs)
     sent = call(
         fix_kernel, (piece,) * 4, [SM] + [VM] * 9, (VM,) * 4, [], 4, 1 << 20, 1 << 18,
-        alias={6 + k: k for k in range(4)}, name="fix",
+        name="fix",
     )(place, earlier, head, head_ids, gate_v, taps_v, *raw)
     parts = [sent[0], None, None, None]
     for d in ORDER:
         parts[d] = lax.ppermute(sent[d], "tp", [(i, (i + d) % tp_count) for i in range(tp_count)])
-    held = (
-        pltpu.VMEM((rows, 2 * tokens), BF16), pltpu.VMEM((2, 2 * tokens, rows), BF16),
-        pltpu.VMEM(out_proj.shape, BF16), pltpu.VMEM(residual_in.shape, BF16), pltpu.VMEM(gain.shape, F32),
-    )
-    onehot, pick, proj_v, residual_v, gain_v = call(
-        slots_kernel, held, [HB] * 4, (VM,) * 5,
-        [pltpu.VMEM((2, tokens), jnp.int32), pltpu.SemaphoreType.DMA((7,))],
-        SLOTS, 1 << 30, 1 << 23, name="slots",
-    )(expert_ids.T, out_proj, residual_in, gain)
+    held = (pltpu.VMEM((rows, 2 * tokens), BF16), pltpu.VMEM((2 * tokens, rows // 2), BF16))
+    onehot, pick = call(
+        slots_kernel, held, [VM], (VM,) * 2, [], SLOTS, SLOT_FLOPS, 1 << 20, name="slots",
+    )(expert_ids.T)
     buf, carried = call(
         mix_kernel, (shape((rows, half), BF16), shape((tokens, width), F32)),
         [SM] + [VM] * 8, (VM, VM),
         [pltpu.VMEM((2 * tokens, half), BF16)],
         12, 8 << 30, 1 << 23, name="mix",
-    )(place, *parts, residual_v, proj_v, gain_v, onehot)
+    )(place, *parts, residual_in, out_proj, gain, onehot)
     arrived = lax.all_to_all(buf.reshape(experts, 8, half), ("sp", "tp"), split_axis=0, concat_axis=0, tiled=True)
     hidden = gate_proj.shape[2]
     result = call(

time: 101 us -> 100 us (0.990)
  Pallas kernels: 15.4 us -> 11.8 us
  waiting for transfers between devices: 0.01 us -> 2.02 us
  blocking collectives: 75.6 us -> 76.7 us
    pallas_call x2, Pallas kernels: 4.12 us -> 1.02 us  [the longest x1 0.51 us: on_device(): call(early_kernel, outs, [SM] + [VM] * 5, (VM,) * len(outs), [pltpu.VMEM(...]
    ppermute x3, waiting for transfers between devices: 0.01 us -> 1.91 us  [on_device(): lax.ppermute(sent[d], 'tp', [(i, (i + d) % tp_count) for i in range(tp_co...]
    all_to_all x1, blocking collectives: 41.4 us -> 42.5 us  [on_device(): lax.all_to_all(buf.reshape(experts, 8, half), ('sp', 'tp'), split_axis=0,...]
  transfers between devices with their start and end apart: 4 -> 4, of which waited for: 0 -> 3; matrix products, arithmetic and copies ran while one was open for 0% -> 0% of each run, Pallas kernels for 4% -> 1%
where the time goes in v4:
time: 100 us
  blocking collectives  76.7 us (77%)
  Pallas kernels  11.8 us (12%)
  starting transfers between devices  9.47 us (9%)
  waiting for transfers between devices  2.02 us (2%)
    all_to_all x1, blocking collectives, on_device(): lax.all_to_all(buf.reshape(experts, 8, half), ('sp', 'tp'), split_axis=0,...  42.5 us
    all_to_all x1, blocking collectives, on_device(): lax.all_to_all(result.reshape(experts, 8, half), ('sp', 'tp'), split_axis...  34.2 us
    pallas_call x1, Pallas kernels, on_device(): call(expert_kernel, shape((rows, half), BF16), [VM] * 4, VM, [pltpu.VMEM(...  6.69 us
    ppermute x3, starting transfers between devices, on_device(): lax.ppermute(sent[d], 'tp', [(i, (i + d) % tp_count) for i in range(tp_co...  4.88 us
    ppermute x1, starting transfers between devices, on_device(): lax.ppermute(edge, 'sp', [(i, i + 1) for i in range(sp_count - 1)])  4.58 us
  transfers between devices with their start and end apart: 4, of which 3 were waited for; matrix products, arithmetic and copies ran while one was open for 0% of the time, Pallas kernels for 1%

profile of v4, /device:TPU:1, one launch (start us, length us, event | category | flops | bytes accessed | tf_op | source)
XLA Modules:
  0.0 100.2 jit_solution(5228256895521824907)
XLA Ops:
  0.0 0.0 copy-start.9
  0.0 0.0 copy-start.10
  0.0 0.9 edge.1
  1.0 4.6 %collective-permute-start = (f32[4,256]{1,0:T(4,128)S(1)}, f32[4,256]{1,0:T(4,128)S(1)}, u32[]{:S(2)}, u32[]{:S(2)}) collective-permute-start(f32[4,256]{1,0:T(4,128)S(1)} %edge.1), channel_id=1, source_target_pairs={{0,4},{4,8},{8,12},{12,16},{16,20},{20,24},{24,28},{28,32},{32,36}... | collective-permute-start | bytes 12296 | tf_op jit(solution)/shard_map/ppermute | solution.py:238
  5.5 0.0 copy-done.5
  5.6 0.0 copy-done.6
  5.6 0.0 copy-done.7
  5.6 0.0 copy-done.9
  5.6 0.0 copy-start.11
  5.6 0.5 early.1
  6.1 0.0 copy-start
  6.1 0.0 copy-start.4
  6.2 0.0 copy-start.8
  6.2 0.1 collective-permute-done.earlier
  6.3 1.3 %collective-permute-start.1 = (bf16[128,256]{1,0:T(8,128)(2,1)S(1)}, bf16[128,256]{1,0:T(8,128)(2,1)S(1)}, u32[]{:S(2)}, u32[]{:S(2)}) collective-permute-start(bf16[128,256]{1,0:T(8,128)(2,1)S(1)} %get-tuple-element.30), channel_id=1, source_target_pairs={{0,1},{1,2},{2,3},{3,0},{4,5},{5,6},{6,7},{7,4},{8,9},{9,10},{10,1... | collective-permute-start | bytes 196616 | tf_op jit(solution)/shard_map/ppermute | solution.py:258
  7.6 2.5 %collective-permute-start.2 = (bf16[128,256]{1,0:T(8,128)(2,1)S(1)}, bf16[128,256]{1,0:T(8,128)(2,1)S(1)}, u32[]{:S(2)}, u32[]{:S(2)}) collective-permute-start(bf16[128,256]{1,0:T(8,128)(2,1)S(1)} %get-tuple-element.31), channel_id=1, source_target_pairs={{0,2},{1,3},{2,0},{3,1},{4,6},{5,7},{6,4},{7,5},{8,10},{9,11},{10,... | collective-permute-start | bytes 196616 | tf_op jit(solution)/shard_map/ppermute | solution.py:258
  10.0 1.2 %collective-permute-start.3 = (bf16[128,256]{1,0:T(8,128)(2,1)S(1)}, bf16[128,256]{1,0:T(8,128)(2,1)S(1)}, u32[]{:S(2)}, u32[]{:S(2)}) collective-permute-start(bf16[128,256]{1,0:T(8,128)(2,1)S(1)} %get-tuple-element.32), channel_id=1, source_target_pairs={{0,3},{1,0},{2,1},{3,2},{4,7},{5,4},{6,5},{7,6},{8,11},{9,8},{10,9... | collective-permute-start | bytes 196616 | tf_op jit(solution)/shard_map/ppermute | solution.py:258
  11.2 0.0 copy-done.11
  11.2 0.5 slots.1
  11.7 0.0 collective-permute-done.1.r1
  11.7 1.4 %collective-permute-done.2.r2 = bf16[128,256]{1,0:T(8,128)(2,1)S(1)} collective-permute-done((bf16[128,256]{1,0:T(8,128)(2,1)S(1)}, bf16[128,256]{1,0:T(8,128)(2,1)S(1)}, u32[]{:S(2)}, u32[]{:S(2)}) %collective-permute-start.2) | collective-permute-done | bytes 65568 | tf_op jit(solution)/shard_map/ppermute | solution.py:258
  13.1 0.6 collective-permute-done.3.r3
  13.6 0.0 copy-done.8
  13.6 0.0 copy-start.2
  13.7 0.0 copy-start.3
  13.7 1.6 %mix.1 = (bf16[1024,1024]{1,0:T(8,128)(2,1)S(1)}, f32[128,2048]{1,0:T(8,128)S(1)}) custom-call(s32[1]{0:T(128)} %bitcast.place, bf16[128,256]{1,0:T(8,128)(2,1)S(1)} %get-tuple-element.29.r0, bf16[128,256]{1,0:T(8,128)(2,1)S(1)} %collective-permute-done.1.r1, bf16[128,256]{1,0:T(8,128)(2,1)S(1)} %collective-permute-done.2.r2, ...), custom_call_target="tpu_custom_call" | custom-call | flops 8589934592 | bytes 8388608 | tf_op jit(solution)/shard_map/mix/pallas_call | solution.py:263
  15.3 0.0 copy-start.1
  15.3 42.5 %all_to_all.10 = bf16[128,8,1024]{2,1,0:T(8,128)(2,1)S(1)} all-to-all(bf16[128,8,1024]{2,1,0:T(8,128)(2,1)S(1)} %bitcast.12), channel_id=1, replica_groups=mesh['sp'=32,'tp'=4] {'sp','tp'}, dimensions={0} | all-to-all | bytes 4194304 | tf_op jit(solution)/shard_map/all_to_all | solution.py:269
  57.8 6.7 %experts.1 = bf16[1024,1024]{1,0:T(8,128)(2,1)S(1)} custom-call(bf16[1024,1024]{1,0:T(8,128)(2,1)S(1)} %bitcast.14, bf16[2048,1024]{1,0:T(8,128)(2,1)S(1)} %bitcast.16, bf16[2048,1024]{1,0:T(8,128)(2,1)S(1)} %bitcast.17, bf16[1024,2048]{1,0:T(8,128)(2,1)S(1)} %bitcast.18), custom_call_target="tpu_custom_call" | custom-call | flops 6442450944 | bytes 16777216 | tf_op jit(solution)/shard_map/experts/pallas_call | solution.py:271
  64.5 0.0 copy-start.12
  64.5 34.2 %all_to_all.11 = bf16[128,8,1024]{2,1,0:T(8,128)(2,1)S(1)} all-to-all(bf16[128,8,1024]{2,1,0:T(8,128)(2,1)S(1)} %bitcast.15), channel_id=1, replica_groups=mesh['sp'=32,'tp'=4] {'sp','tp'}, dimensions={0} | all-to-all | bytes 4194304 | tf_op jit(solution)/shard_map/all_to_all | solution.py:279
  98.7 1.6 %combine.1 = bf16[128,2048]{1,0:T(8,128)(2,1)} custom-call(bf16[1024,1024]{1,0:T(8,128)(2,1)S(1)} %bitcast.13, f32[128,2048]{1,0:T(8,128)S(1)} %get-tuple-element.35.carried, bf16[256,512]{1,0:T(8,128)(2,1)S(1)} %get-tuple-element.36.pick, f32[2,128]{1,0:T(2,128)S(1)} %bitcast.23), custom_call_target="tpu_custom_call" | custom-call | flops 1073741824 | bytes 4194304 | tf_op jit(solution)/shard_map/combine/pallas_call | solution.py:280
  (11 shorter events, 0.0 us)
Async XLA Ops:
  0.0 5.5 %copy-start.5 = (bf16[512,256]{1,0:T(8,128)(2,1)S(1)}, bf16[512,256]{1,0:T(8,128)(2,1)}, u32[]{:S(2)}) copy-start(bf16[512,256]{1,0:T(8,128)(2,1)} %xv.1) | copy-start | bytes 786436
  0.0 5.6 %copy-start.6 = (bf16[512,256]{1,0:T(8,128)(2,1)S(1)}, bf16[512,256]{1,0:T(8,128)(2,1)}, u32[]{:S(2)}) copy-start(bf16[512,256]{1,0:T(8,128)(2,1)} %gv.1) | copy-start | bytes 786436
  0.0 5.6 %copy-start.7 = (bf16[512,256]{1,0:T(8,128)(2,1)S(1)}, bf16[512,256]{1,0:T(8,128)(2,1)}, u32[]{:S(2)}) copy-start(bf16[512,256]{1,0:T(8,128)(2,1)} %ov.1) | copy-start | bytes 786436
  0.0 5.6 %copy-start.9 = (s32[512]{0:T(512)S(1)}, s32[512]{0:T(512)}, u32[]{:S(2)}) copy-start(s32[512]{0:T(512)} %param.17) | copy-start | bytes 6148
  0.0 5.6 %copy-start.10 = (bf16[3,256]{1,0:T(4,128)(2,1)S(1)}, bf16[3,256]{1,0:T(4,128)(2,1)}, u32[]{:S(2)}) copy-start(bf16[3,256]{1,0:T(4,128)(2,1)} %taps.1) | copy-start | bytes 4612
  1.0 5.3 %collective-permute-start = (f32[4,256]{1,0:T(4,128)S(1)}, f32[4,256]{1,0:T(4,128)S(1)}, u32[]{:S(2)}, u32[]{:S(2)}) collective-permute-start(f32[4,256]{1,0:T(4,128)S(1)} %edge.1), channel_id=1, source_target_pairs={{0,4},{4,8},{8,12},{12,16},{16,20},{20,24},{24,28},{28,32},{32,36}... | collective-permute-start | bytes 12296 | tf_op jit(solution)/shard_map/ppermute | solution.py:238
  5.6 5.6 %copy-start.11 = (s32[128,2]{0,1:T(2,128)S(1)}, s32[128,2]{0,1:T(2,128)}, u32[]{:S(2)}) copy-start(s32[128,2]{0,1:T(2,128)} %param.21) | copy-start | bytes 3076
  6.1 7.5 %copy-start = (bf16[1024,2048]{1,0:T(8,128)(2,1)S(1)}, bf16[1024,2048]{1,0:T(8,128)(2,1)}, u32[]{:S(2)}) copy-start(bf16[1024,2048]{1,0:T(8,128)(2,1)} %proj.1) | copy-start | bytes 12582916
  6.1 7.5 %copy-start.4 = (bf16[128,2048]{1,0:T(8,128)(2,1)S(1)}, bf16[128,2048]{1,0:T(8,128)(2,1)}, u32[]{:S(2)}) copy-start(bf16[128,2048]{1,0:T(8,128)(2,1)} %residual.1) | copy-start | bytes 1572868
  6.2 7.5 %copy-start.8 = (f32[2048]{0:T(1024)S(1)}, f32[2048]{0:T(1024)}, u32[]{:S(2)}) copy-start(f32[2048]{0:T(1024)} %param.20) | copy-start | bytes 24580
  6.3 5.4 %collective-permute-start.1 = (bf16[128,256]{1,0:T(8,128)(2,1)S(1)}, bf16[128,256]{1,0:T(8,128)(2,1)S(1)}, u32[]{:S(2)}, u32[]{:S(2)}) collective-permute-start(bf16[128,256]{1,0:T(8,128)(2,1)S(1)} %get-tuple-element.30), channel_id=1, source_target_pairs={{0,1},{1,2},{2,3},{3,0},{4,5},{5,6},{6,7},{7,4},{8,9},{9,10},{10,1... | collective-permute-start | bytes 196616 | tf_op jit(solution)/shard_map/ppermute | solution.py:258
  7.6 5.5 %collective-permute-start.2 = (bf16[128,256]{1,0:T(8,128)(2,1)S(1)}, bf16[128,256]{1,0:T(8,128)(2,1)S(1)}, u32[]{:S(2)}, u32[]{:S(2)}) collective-permute-start(bf16[128,256]{1,0:T(8,128)(2,1)S(1)} %get-tuple-element.31), channel_id=1, source_target_pairs={{0,2},{1,3},{2,0},{3,1},{4,6},{5,7},{6,4},{7,5},{8,10},{9,11},{10,... | collective-permute-start | bytes 196616 | tf_op jit(solution)/shard_map/ppermute | solution.py:258
  10.0 3.6 %collective-permute-start.3 = (bf16[128,256]{1,0:T(8,128)(2,1)S(1)}, bf16[128,256]{1,0:T(8,128)(2,1)S(1)}, u32[]{:S(2)}, u32[]{:S(2)}) collective-permute-start(bf16[128,256]{1,0:T(8,128)(2,1)S(1)} %get-tuple-element.32), channel_id=1, source_target_pairs={{0,3},{1,0},{2,1},{3,2},{4,7},{5,4},{6,5},{7,6},{8,11},{9,8},{10,9... | collective-permute-start | bytes 196616 | tf_op jit(solution)/shard_map/ppermute | solution.py:258
  13.6 44.2 %copy-start.2 = (bf16[1,2048,1024]{2,1,0:T(8,128)(2,1)S(1)}, bf16[1,2048,1024]{2,1,0:T(8,128)(2,1)}, u32[]{:S(2)}) copy-start(bf16[1,2048,1024]{2,1,0:T(8,128)(2,1)} %param.24) | copy-start | bytes 12582916
  13.7 44.2 %copy-start.3 = (bf16[1,1024,2048]{2,1,0:T(8,128)(2,1)S(1)}, bf16[1,1024,2048]{2,1,0:T(8,128)(2,1)}, u32[]{:S(2)}) copy-start(bf16[1,1024,2048]{2,1,0:T(8,128)(2,1)} %param.25) | copy-start | bytes 12582916
  15.3 42.5 %copy-start.1 = (bf16[1,2048,1024]{2,1,0:T(8,128)(2,1)S(1)}, bf16[1,2048,1024]{2,1,0:T(8,128)(2,1)}, u32[]{:S(2)}) copy-start(bf16[1,2048,1024]{2,1,0:T(8,128)(2,1)} %param.23) | copy-start | bytes 12582916
  64.5 34.2 %copy-start.12 = (f32[128,2]{0,1:T(2,128)S(1)}, f32[128,2]{0,1:T(2,128)}, u32[]{:S(2)}) copy-start(f32[128,2]{0,1:T(2,128)} %param.22) | copy-start | bytes 3076

commit v5 on v4

--- a/solution.py
+++ b/solution.py
@@ -37,10 +37,9 @@
         copy.wait()
     prod = xv[...].astype(F32) * gv[...].astype(F32)
     last = dv.shape[0] - 1
-    ids = jnp.broadcast_to(dv[last : last + 1, :].astype(F32), (128, 128)).T
     out[0:2, :] = prod[14:16, :]
     for c in range(out.shape[1] // 128):
-        out[2:4, 128 * c : 128 * c + 128] = ids[126:128, :]
+        out[2:4, 128 * c : 128 * c + 128] = jnp.broadcast_to(dv[last : last + 1, :].astype(F32), (2, 128))
 
 
 def taps_of(taps):
@@ -117,7 +116,8 @@
     part = i0.shape[0]
     here = place[0]
     window = jnp.concatenate([jnp.zeros((6, width), F32), earlier[0:2, :], head[...]], axis=0)
-    ids = jnp.concatenate([jnp.zeros((6, 128), F32), earlier[2:4, 0:128], head_ids[...]], axis=0)
+    before = [jnp.broadcast_to(earlier[2:3, k : k + 1], (1, 128)) for k in (126, 127)]
+    ids = jnp.concatenate([jnp.zeros((6, 128), F32), *before, head_ids[...]], axis=0)
     pieces = conv_rows(window, ids, g_out[...], taps_of(taps))
     for shift, (old, out) in enumerate(zip((i0, i1, i2, i3), (o0, o1, o2, o3))):
         out[16:part, :] = old[16:part, :]

time: 100 us -> 100 us (level)
  no operation moved by 1% of the time
where the time goes in v5:
time: 100 us
  blocking collectives  76.7 us (77%)
  Pallas kernels  11.8 us (12%)
  starting transfers between devices  9.47 us (9%)
  waiting for transfers between devices  2.03 us (2%)
    all_to_all x1, blocking collectives, on_device(): lax.all_to_all(buf.reshape(experts, 8, half), ('sp', 'tp'), split_axis=0,...  42.5 us
    all_to_all x1, blocking collectives, on_device(): lax.all_to_all(result.reshape(experts, 8, half), ('sp', 'tp'), split_axis...  34.2 us
    pallas_call x1, Pallas kernels, on_device(): call(expert_kernel, shape((rows, half), BF16), [VM] * 4, VM, [pltpu.VMEM(...  6.69 us
    ppermute x3, starting transfers between devices, on_device(): lax.ppermute(sent[d], 'tp', [(i, (i + d) % tp_count) for i in range(tp_co...  4.88 us
    ppermute x1, starting transfers between devices, on_device(): lax.ppermute(edge, 'sp', [(i, i + 1) for i in range(sp_count - 1)])  4.58 us
  transfers between devices with their start and end apart: 4, of which 3 were waited for; matrix products, arithmetic and copies ran while one was open for 0% of the time, Pallas kernels for 1%

profile of v5, /device:TPU:1, one launch (start us, length us, event | category | flops | bytes accessed | tf_op | source)
XLA Modules:
  0.0 100.2 jit_solution(13761195474386412772)
XLA Ops:
  0.0 0.0 copy-start.9
  0.0 0.0 copy-start.10
  0.0 0.8 edge.1
  0.9 4.6 %collective-permute-start = (f32[4,256]{1,0:T(4,128)S(1)}, f32[4,256]{1,0:T(4,128)S(1)}, u32[]{:S(2)}, u32[]{:S(2)}) collective-permute-start(f32[4,256]{1,0:T(4,128)S(1)} %edge.1), channel_id=1, source_target_pairs={{0,4},{4,8},{8,12},{12,16},{16,20},{20,24},{24,28},{28,32},{32,36}... | collective-permute-start | bytes 12296 | tf_op jit(solution)/shard_map/ppermute | solution.py:238
  5.4 0.0 copy-done.5
  5.5 0.0 copy-done.6
  5.5 0.0 copy-start.11
  5.5 0.5 early.1
  6.0 0.0 copy-start
  6.0 0.0 copy-start.4
  6.1 0.0 copy-start.8
  6.1 0.1 collective-permute-done.earlier
  6.2 0.1 fix.1
  6.3 1.3 %collective-permute-start.1 = (bf16[128,256]{1,0:T(8,128)(2,1)S(1)}, bf16[128,256]{1,0:T(8,128)(2,1)S(1)}, u32[]{:S(2)}, u32[]{:S(2)}) collective-permute-start(bf16[128,256]{1,0:T(8,128)(2,1)S(1)} %get-tuple-element.30), channel_id=1, source_target_pairs={{0,1},{1,2},{2,3},{3,0},{4,5},{5,6},{6,7},{7,4},{8,9},{9,10},{10,1... | collective-permute-start | bytes 196616 | tf_op jit(solution)/shard_map/ppermute | solution.py:258
  7.5 2.5 %collective-permute-start.2 = (bf16[128,256]{1,0:T(8,128)(2,1)S(1)}, bf16[128,256]{1,0:T(8,128)(2,1)S(1)}, u32[]{:S(2)}, u32[]{:S(2)}) collective-permute-start(bf16[128,256]{1,0:T(8,128)(2,1)S(1)} %get-tuple-element.31), channel_id=1, source_target_pairs={{0,2},{1,3},{2,0},{3,1},{4,6},{5,7},{6,4},{7,5},{8,10},{9,11},{10,... | collective-permute-start | bytes 196616 | tf_op jit(solution)/shard_map/ppermute | solution.py:258
  10.0 1.2 %collective-permute-start.3 = (bf16[128,256]{1,0:T(8,128)(2,1)S(1)}, bf16[128,256]{1,0:T(8,128)(2,1)S(1)}, u32[]{:S(2)}, u32[]{:S(2)}) collective-permute-start(bf16[128,256]{1,0:T(8,128)(2,1)S(1)} %get-tuple-element.32), channel_id=1, source_target_pairs={{0,3},{1,0},{2,1},{3,2},{4,7},{5,4},{6,5},{7,6},{8,11},{9,8},{10,9... | collective-permute-start | bytes 196616 | tf_op jit(solution)/shard_map/ppermute | solution.py:258
  11.1 0.0 copy-done.11
  11.2 0.5 slots.1
  11.7 0.0 collective-permute-done.1.r1
  11.7 1.4 %collective-permute-done.2.r2 = bf16[128,256]{1,0:T(8,128)(2,1)S(1)} collective-permute-done((bf16[128,256]{1,0:T(8,128)(2,1)S(1)}, bf16[128,256]{1,0:T(8,128)(2,1)S(1)}, u32[]{:S(2)}, u32[]{:S(2)}) %collective-permute-start.2) | collective-permute-done | bytes 65568 | tf_op jit(solution)/shard_map/ppermute | solution.py:258
  13.0 0.6 collective-permute-done.3.r3
  13.6 0.0 copy-start.2
  13.6 0.0 copy-start.3
  13.6 1.6 %mix.1 = (bf16[1024,1024]{1,0:T(8,128)(2,1)S(1)}, f32[128,2048]{1,0:T(8,128)S(1)}) custom-call(s32[1]{0:T(128)} %bitcast.place, bf16[128,256]{1,0:T(8,128)(2,1)S(1)} %get-tuple-element.29.r0, bf16[128,256]{1,0:T(8,128)(2,1)S(1)} %collective-permute-done.1.r1, bf16[128,256]{1,0:T(8,128)(2,1)S(1)} %collective-permute-done.2.r2, ...), custom_call_target="tpu_custom_call" | custom-call | flops 8589934592 | bytes 8388608 | tf_op jit(solution)/shard_map/mix/pallas_call | solution.py:263
  15.2 0.0 copy-start.1
  15.3 42.5 %all_to_all.10 = bf16[128,8,1024]{2,1,0:T(8,128)(2,1)S(1)} all-to-all(bf16[128,8,1024]{2,1,0:T(8,128)(2,1)S(1)} %bitcast.12), channel_id=1, replica_groups=mesh['sp'=32,'tp'=4] {'sp','tp'}, dimensions={0} | all-to-all | bytes 4194304 | tf_op jit(solution)/shard_map/all_to_all | solution.py:269
  57.8 0.0 copy-done.2
  57.8 0.0 copy-done.1
  57.8 6.7 %experts.1 = bf16[1024,1024]{1,0:T(8,128)(2,1)S(1)} custom-call(bf16[1024,1024]{1,0:T(8,128)(2,1)S(1)} %bitcast.14, bf16[2048,1024]{1,0:T(8,128)(2,1)S(1)} %bitcast.16, bf16[2048,1024]{1,0:T(8,128)(2,1)S(1)} %bitcast.17, bf16[1024,2048]{1,0:T(8,128)(2,1)S(1)} %bitcast.18), custom_call_target="tpu_custom_call" | custom-call | flops 6442450944 | bytes 16777216 | tf_op jit(solution)/shard_map/experts/pallas_call | solution.py:271
  64.5 0.0 copy-start.12
  64.5 34.2 %all_to_all.11 = bf16[128,8,1024]{2,1,0:T(8,128)(2,1)S(1)} all-to-all(bf16[128,8,1024]{2,1,0:T(8,128)(2,1)S(1)} %bitcast.15), channel_id=1, replica_groups=mesh['sp'=32,'tp'=4] {'sp','tp'}, dimensions={0} | all-to-all | bytes 4194304 | tf_op jit(solution)/shard_map/all_to_all | solution.py:279
  98.6 1.6 %combine.1 = bf16[128,2048]{1,0:T(8,128)(2,1)} custom-call(bf16[1024,1024]{1,0:T(8,128)(2,1)S(1)} %bitcast.13, f32[128,2048]{1,0:T(8,128)S(1)} %get-tuple-element.35.carried, bf16[256,512]{1,0:T(8,128)(2,1)S(1)} %get-tuple-element.36.pick, f32[2,128]{1,0:T(2,128)S(1)} %bitcast.23), custom_call_target="tpu_custom_call" | custom-call | flops 1073741824 | bytes 4194304 | tf_op jit(solution)/shard_map/combine/pallas_call | solution.py:280
  (11 shorter events, 0.0 us)
Async XLA Ops:
  0.0 5.4 %copy-start.5 = (bf16[512,256]{1,0:T(8,128)(2,1)S(1)}, bf16[512,256]{1,0:T(8,128)(2,1)}, u32[]{:S(2)}) copy-start(bf16[512,256]{1,0:T(8,128)(2,1)} %xv.1) | copy-start | bytes 786436
  0.0 5.5 %copy-start.6 = (bf16[512,256]{1,0:T(8,128)(2,1)S(1)}, bf16[512,256]{1,0:T(8,128)(2,1)}, u32[]{:S(2)}) copy-start(bf16[512,256]{1,0:T(8,128)(2,1)} %gv.1) | copy-start | bytes 786436
  0.0 5.5 %copy-start.7 = (bf16[512,256]{1,0:T(8,128)(2,1)S(1)}, bf16[512,256]{1,0:T(8,128)(2,1)}, u32[]{:S(2)}) copy-start(bf16[512,256]{1,0:T(8,128)(2,1)} %ov.1) | copy-start | bytes 786436
  0.0 5.5 %copy-start.9 = (s32[512]{0:T(512)S(1)}, s32[512]{0:T(512)}, u32[]{:S(2)}) copy-start(s32[512]{0:T(512)} %param.17) | copy-start | bytes 6148
  0.0 5.5 %copy-start.10 = (bf16[3,256]{1,0:T(4,128)(2,1)S(1)}, bf16[3,256]{1,0:T(4,128)(2,1)}, u32[]{:S(2)}) copy-start(bf16[3,256]{1,0:T(4,128)(2,1)} %taps.1) | copy-start | bytes 4612
  0.9 5.3 %collective-permute-start = (f32[4,256]{1,0:T(4,128)S(1)}, f32[4,256]{1,0:T(4,128)S(1)}, u32[]{:S(2)}, u32[]{:S(2)}) collective-permute-start(f32[4,256]{1,0:T(4,128)S(1)} %edge.1), channel_id=1, source_target_pairs={{0,4},{4,8},{8,12},{12,16},{16,20},{20,24},{24,28},{28,32},{32,36}... | collective-permute-start | bytes 12296 | tf_op jit(solution)/shard_map/ppermute | solution.py:238
  5.5 5.7 %copy-start.11 = (s32[128,2]{0,1:T(2,128)S(1)}, s32[128,2]{0,1:T(2,128)}, u32[]{:S(2)}) copy-start(s32[128,2]{0,1:T(2,128)} %param.21) | copy-start | bytes 3076
  6.0 7.6 %copy-start = (bf16[1024,2048]{1,0:T(8,128)(2,1)S(1)}, bf16[1024,2048]{1,0:T(8,128)(2,1)}, u32[]{:S(2)}) copy-start(bf16[1024,2048]{1,0:T(8,128)(2,1)} %proj.1) | copy-start | bytes 12582916
  6.0 7.5 %copy-start.4 = (bf16[128,2048]{1,0:T(8,128)(2,1)S(1)}, bf16[128,2048]{1,0:T(8,128)(2,1)}, u32[]{:S(2)}) copy-start(bf16[128,2048]{1,0:T(8,128)(2,1)} %residual.1) | copy-start | bytes 1572868
  6.1 7.5 %copy-start.8 = (f32[2048]{0:T(1024)S(1)}, f32[2048]{0:T(1024)}, u32[]{:S(2)}) copy-start(f32[2048]{0:T(1024)} %param.20) | copy-start | bytes 24580
  6.3 5.4 %collective-permute-start.1 = (bf16[128,256]{1,0:T(8,128)(2,1)S(1)}, bf16[128,256]{1,0:T(8,128)(2,1)S(1)}, u32[]{:S(2)}, u32[]{:S(2)}) collective-permute-start(bf16[128,256]{1,0:T(8,128)(2,1)S(1)} %get-tuple-element.30), channel_id=1, source_target_pairs={{0,1},{1,2},{2,3},{3,0},{4,5},{5,6},{6,7},{7,4},{8,9},{9,10},{10,1... | collective-permute-start | bytes 196616 | tf_op jit(solution)/shard_map/ppermute | solution.py:258
  7.5 5.5 %collective-permute-start.2 = (bf16[128,256]{1,0:T(8,128)(2,1)S(1)}, bf16[128,256]{1,0:T(8,128)(2,1)S(1)}, u32[]{:S(2)}, u32[]{:S(2)}) collective-permute-start(bf16[128,256]{1,0:T(8,128)(2,1)S(1)} %get-tuple-element.31), channel_id=1, source_target_pairs={{0,2},{1,3},{2,0},{3,1},{4,6},{5,7},{6,4},{7,5},{8,10},{9,11},{10,... | collective-permute-start | bytes 196616 | tf_op jit(solution)/shard_map/ppermute | solution.py:258
  10.0 3.6 %collective-permute-start.3 = (bf16[128,256]{1,0:T(8,128)(2,1)S(1)}, bf16[128,256]{1,0:T(8,128)(2,1)S(1)}, u32[]{:S(2)}, u32[]{:S(2)}) collective-permute-start(bf16[128,256]{1,0:T(8,128)(2,1)S(1)} %get-tuple-element.32), channel_id=1, source_target_pairs={{0,3},{1,0},{2,1},{3,2},{4,7},{5,4},{6,5},{7,6},{8,11},{9,8},{10,9... | collective-permute-start | bytes 196616 | tf_op jit(solution)/shard_map/ppermute | solution.py:258
  13.6 44.2 %copy-start.2 = (bf16[1,2048,1024]{2,1,0:T(8,128)(2,1)S(1)}, bf16[1,2048,1024]{2,1,0:T(8,128)(2,1)}, u32[]{:S(2)}) copy-start(bf16[1,2048,1024]{2,1,0:T(8,128)(2,1)} %param.24) | copy-start | bytes 12582916
  13.6 44.2 %copy-start.3 = (bf16[1,1024,2048]{2,1,0:T(8,128)(2,1)S(1)}, bf16[1,1024,2048]{2,1,0:T(8,128)(2,1)}, u32[]{:S(2)}) copy-start(bf16[1,1024,2048]{2,1,0:T(8,128)(2,1)} %param.25) | copy-start | bytes 12582916
  15.2 42.5 %copy-start.1 = (bf16[1,2048,1024]{2,1,0:T(8,128)(2,1)S(1)}, bf16[1,2048,1024]{2,1,0:T(8,128)(2,1)}, u32[]{:S(2)}) copy-start(bf16[1,2048,1024]{2,1,0:T(8,128)(2,1)} %param.23) | copy-start | bytes 12582916
  64.5 34.2 %copy-start.12 = (f32[128,2]{0,1:T(2,128)S(1)}, f32[128,2]{0,1:T(2,128)}, u32[]{:S(2)}) copy-start(f32[128,2]{0,1:T(2,128)} %param.22) | copy-start | bytes 3076

commit v6 on v5

--- a/solution.py
+++ b/solution.py
@@ -127,21 +127,20 @@
             out[0:16, c] = jnp.where(mine, piece.astype(F32), old[0:16, c].astype(F32)).astype(BF16)
 
 
-def mix_kernel(place, r0, r1, r2, r3, residual, proj, gain, onehot, buf, carried, halves):
+def mix_kernel(place, r0, r1, r2, r3, residual, proj, gain, onehot, buf, carried, halves, joined):
     here = place[0]
     width = residual.shape[1]
     half = width // 2
     tokens = residual.shape[0]
+    for shift, part in enumerate((r0, r1, r2, r3)):
+        depth = part.shape[1]
+        start = pl.multiple_of(lax.rem(here + 4 - shift, 4) * depth, depth)
+        joined[:, pl.ds(start, depth)] = part[...]
     step = 512
     total = jnp.zeros((tokens, 1), F32)
     for n in range(width // step):
         c = slice(n * step, n * step + step)
-        acc = None
-        for shift, part in enumerate((r0, r1, r2, r3)):
-            depth = part.shape[1]
-            start = pl.multiple_of(lax.rem(here + 4 - shift, 4) * depth, depth)
-            term = dot(part[...], proj[pl.ds(start, depth), c])
-            acc = term if acc is None else acc + term
+        acc = dot(joined[...], proj[:, c])
         value = residual[:, c].astype(F32) + acc.astype(BF16).astype(F32)
         carried[:, c] = value
         total = total + jnp.sum(value * value, axis=1, keepdims=True)
@@ -263,7 +262,7 @@
     buf, carried = call(
         mix_kernel, (shape((rows, half), BF16), shape((tokens, width), F32)),
         [SM] + [VM] * 8, (VM, VM),
-        [pltpu.VMEM((2 * tokens, half), BF16)],
+        [pltpu.VMEM((2 * tokens, half), BF16), pltpu.VMEM((tokens, out_proj.shape[0]), BF16)],
         12, 8 << 30, 1 << 23, name="mix",
     )(place, *parts, residual_in, out_proj, gain, onehot)
     arrived = lax.all_to_all(buf.reshape(experts, 8, half), ("sp", "tp"), split_axis=0, concat_axis=0, tiled=True)

time: 100 us -> 100 us (level)
  no operation moved by 1% of the time
where the time goes in v6:
time: 100 us
  blocking collectives  76.7 us (77%)
  Pallas kernels  11.8 us (12%)
  starting transfers between devices  9.47 us (9%)
  waiting for transfers between devices  2.03 us (2%)
    all_to_all x1, blocking collectives, on_device(): lax.all_to_all(buf.reshape(experts, 8, half), ('sp', 'tp'), split_axis=0,...  42.5 us
    all_to_all x1, blocking collectives, on_device(): lax.all_to_all(result.reshape(experts, 8, half), ('sp', 'tp'), split_axis...  34.2 us
    pallas_call x1, Pallas kernels, on_device(): call(expert_kernel, shape((rows, half), BF16), [VM] * 4, VM, [pltpu.VMEM(...  6.69 us
    ppermute x3, starting transfers between devices, on_device(): lax.ppermute(sent[d], 'tp', [(i, (i + d) % tp_count) for i in range(tp_co...  4.88 us
    ppermute x1, starting transfers between devices, on_device(): lax.ppermute(edge, 'sp', [(i, i + 1) for i in range(sp_count - 1)])  4.58 us
  transfers between devices with their start and end apart: 4, of which 3 were waited for; matrix products, arithmetic and copies ran while one was open for 0% of the time, Pallas kernels for 1%

profile of v6, /device:TPU:1, one launch (start us, length us, event | category | flops | bytes accessed | tf_op | source)
XLA Modules:
  0.0 100.2 jit_solution(6210852123552491948)
XLA Ops:
  0.0 0.0 copy-start.9
  0.0 0.0 copy-start.10
  0.0 0.8 edge.1
  0.9 4.6 %collective-permute-start = (f32[4,256]{1,0:T(4,128)S(1)}, f32[4,256]{1,0:T(4,128)S(1)}, u32[]{:S(2)}, u32[]{:S(2)}) collective-permute-start(f32[4,256]{1,0:T(4,128)S(1)} %edge.1), channel_id=1, source_target_pairs={{0,4},{4,8},{8,12},{12,16},{16,20},{20,24},{24,28},{28,32},{32,36}... | collective-permute-start | bytes 12296 | tf_op jit(solution)/shard_map/ppermute | solution.py:237
  5.4 0.0 copy-done.5
  5.5 0.0 copy-done.6
  5.5 0.0 copy-done.7
  5.5 0.0 copy-done.9
  5.5 0.0 copy-done.10
  5.5 0.0 copy-start.11
  5.5 0.5 early.1
  6.0 0.0 copy-start
  6.0 0.0 copy-start.4
  6.1 0.0 copy-start.8
  6.1 0.1 collective-permute-done.earlier
  6.2 0.1 fix.1
  6.3 1.3 %collective-permute-start.1 = (bf16[128,256]{1,0:T(8,128)(2,1)S(1)}, bf16[128,256]{1,0:T(8,128)(2,1)S(1)}, u32[]{:S(2)}, u32[]{:S(2)}) collective-permute-start(bf16[128,256]{1,0:T(8,128)(2,1)S(1)} %get-tuple-element.30), channel_id=1, source_target_pairs={{0,1},{1,2},{2,3},{3,0},{4,5},{5,6},{6,7},{7,4},{8,9},{9,10},{10,1... | collective-permute-start | bytes 196616 | tf_op jit(solution)/shard_map/ppermute | solution.py:257
  7.5 2.5 %collective-permute-start.2 = (bf16[128,256]{1,0:T(8,128)(2,1)S(1)}, bf16[128,256]{1,0:T(8,128)(2,1)S(1)}, u32[]{:S(2)}, u32[]{:S(2)}) collective-permute-start(bf16[128,256]{1,0:T(8,128)(2,1)S(1)} %get-tuple-element.31), channel_id=1, source_target_pairs={{0,2},{1,3},{2,0},{3,1},{4,6},{5,7},{6,4},{7,5},{8,10},{9,11},{10,... | collective-permute-start | bytes 196616 | tf_op jit(solution)/shard_map/ppermute | solution.py:257
  10.0 1.2 %collective-permute-start.3 = (bf16[128,256]{1,0:T(8,128)(2,1)S(1)}, bf16[128,256]{1,0:T(8,128)(2,1)S(1)}, u32[]{:S(2)}, u32[]{:S(2)}) collective-permute-start(bf16[128,256]{1,0:T(8,128)(2,1)S(1)} %get-tuple-element.32), channel_id=1, source_target_pairs={{0,3},{1,0},{2,1},{3,2},{4,7},{5,4},{6,5},{7,6},{8,11},{9,8},{10,9... | collective-permute-start | bytes 196616 | tf_op jit(solution)/shard_map/ppermute | solution.py:257
  11.2 0.5 slots.1
  11.7 0.0 collective-permute-done.1.r1
  11.7 1.4 %collective-permute-done.2.r2 = bf16[128,256]{1,0:T(8,128)(2,1)S(1)} collective-permute-done((bf16[128,256]{1,0:T(8,128)(2,1)S(1)}, bf16[128,256]{1,0:T(8,128)(2,1)S(1)}, u32[]{:S(2)}, u32[]{:S(2)}) %collective-permute-start.2) | collective-permute-done | bytes 65568 | tf_op jit(solution)/shard_map/ppermute | solution.py:257
  13.0 0.6 collective-permute-done.3.r3
  13.6 0.0 copy-start.2
  13.6 0.0 copy-start.3
  13.6 1.6 %mix.1 = (bf16[1024,1024]{1,0:T(8,128)(2,1)S(1)}, f32[128,2048]{1,0:T(8,128)S(1)}) custom-call(s32[1]{0:T(128)} %bitcast.place, bf16[128,256]{1,0:T(8,128)(2,1)S(1)} %get-tuple-element.29.r0, bf16[128,256]{1,0:T(8,128)(2,1)S(1)} %collective-permute-done.1.r1, bf16[128,256]{1,0:T(8,128)(2,1)S(1)} %collective-permute-done.2.r2, ...), custom_call_target="tpu_custom_call" | custom-call | flops 8589934592 | bytes 8388608 | tf_op jit(solution)/shard_map/mix/pallas_call | solution.py:262
  15.3 0.0 copy-start.1
  15.3 42.5 %all_to_all.10 = bf16[128,8,1024]{2,1,0:T(8,128)(2,1)S(1)} all-to-all(bf16[128,8,1024]{2,1,0:T(8,128)(2,1)S(1)} %bitcast.12), channel_id=1, replica_groups=mesh['sp'=32,'tp'=4] {'sp','tp'}, dimensions={0} | all-to-all | bytes 4194304 | tf_op jit(solution)/shard_map/all_to_all | solution.py:268
  57.8 6.7 %experts.1 = bf16[1024,1024]{1,0:T(8,128)(2,1)S(1)} custom-call(bf16[1024,1024]{1,0:T(8,128)(2,1)S(1)} %bitcast.14, bf16[2048,1024]{1,0:T(8,128)(2,1)S(1)} %bitcast.16, bf16[2048,1024]{1,0:T(8,128)(2,1)S(1)} %bitcast.17, bf16[1024,2048]{1,0:T(8,128)(2,1)S(1)} %bitcast.18), custom_call_target="tpu_custom_call" | custom-call | flops 6442450944 | bytes 16777216 | tf_op jit(solution)/shard_map/experts/pallas_call | solution.py:270
  64.5 0.0 copy-start.12
  64.5 34.2 %all_to_all.11 = bf16[128,8,1024]{2,1,0:T(8,128)(2,1)S(1)} all-to-all(bf16[128,8,1024]{2,1,0:T(8,128)(2,1)S(1)} %bitcast.15), channel_id=1, replica_groups=mesh['sp'=32,'tp'=4] {'sp','tp'}, dimensions={0} | all-to-all | bytes 4194304 | tf_op jit(solution)/shard_map/all_to_all | solution.py:278
  98.7 1.6 %combine.1 = bf16[128,2048]{1,0:T(8,128)(2,1)} custom-call(bf16[1024,1024]{1,0:T(8,128)(2,1)S(1)} %bitcast.13, f32[128,2048]{1,0:T(8,128)S(1)} %get-tuple-element.35.carried, bf16[256,512]{1,0:T(8,128)(2,1)S(1)} %get-tuple-element.36.pick, f32[2,128]{1,0:T(2,128)S(1)} %bitcast.23), custom_call_target="tpu_custom_call" | custom-call | flops 1073741824 | bytes 4194304 | tf_op jit(solution)/shard_map/combine/pallas_call | solution.py:279
  (11 shorter events, 0.0 us)
Async XLA Ops:
  0.0 5.4 %copy-start.5 = (bf16[512,256]{1,0:T(8,128)(2,1)S(1)}, bf16[512,256]{1,0:T(8,128)(2,1)}, u32[]{:S(2)}) copy-start(bf16[512,256]{1,0:T(8,128)(2,1)} %xv.1) | copy-start | bytes 786436
  0.0 5.5 %copy-start.6 = (bf16[512,256]{1,0:T(8,128)(2,1)S(1)}, bf16[512,256]{1,0:T(8,128)(2,1)}, u32[]{:S(2)}) copy-start(bf16[512,256]{1,0:T(8,128)(2,1)} %gv.1) | copy-start | bytes 786436
  0.0 5.5 %copy-start.7 = (bf16[512,256]{1,0:T(8,128)(2,1)S(1)}, bf16[512,256]{1,0:T(8,128)(2,1)}, u32[]{:S(2)}) copy-start(bf16[512,256]{1,0:T(8,128)(2,1)} %ov.1) | copy-start | bytes 786436
  0.0 5.5 %copy-start.9 = (s32[512]{0:T(512)S(1)}, s32[512]{0:T(512)}, u32[]{:S(2)}) copy-start(s32[512]{0:T(512)} %param.17) | copy-start | bytes 6148
  0.0 5.5 %copy-start.10 = (bf16[3,256]{1,0:T(4,128)(2,1)S(1)}, bf16[3,256]{1,0:T(4,128)(2,1)}, u32[]{:S(2)}) copy-start(bf16[3,256]{1,0:T(4,128)(2,1)} %taps.1) | copy-start | bytes 4612
  0.9 5.3 %collective-permute-start = (f32[4,256]{1,0:T(4,128)S(1)}, f32[4,256]{1,0:T(4,128)S(1)}, u32[]{:S(2)}, u32[]{:S(2)}) collective-permute-start(f32[4,256]{1,0:T(4,128)S(1)} %edge.1), channel_id=1, source_target_pairs={{0,4},{4,8},{8,12},{12,16},{16,20},{20,24},{24,28},{28,32},{32,36}... | collective-permute-start | bytes 12296 | tf_op jit(solution)/shard_map/ppermute | solution.py:237
  5.5 5.7 %copy-start.11 = (s32[128,2]{0,1:T(2,128)S(1)}, s32[128,2]{0,1:T(2,128)}, u32[]{:S(2)}) copy-start(s32[128,2]{0,1:T(2,128)} %param.21) | copy-start | bytes 3076
  6.0 7.6 %copy-start = (bf16[1024,2048]{1,0:T(8,128)(2,1)S(1)}, bf16[1024,2048]{1,0:T(8,128)(2,1)}, u32[]{:S(2)}) copy-start(bf16[1024,2048]{1,0:T(8,128)(2,1)} %proj.1) | copy-start | bytes 12582916
  6.0 7.5 %copy-start.4 = (bf16[128,2048]{1,0:T(8,128)(2,1)S(1)}, bf16[128,2048]{1,0:T(8,128)(2,1)}, u32[]{:S(2)}) copy-start(bf16[128,2048]{1,0:T(8,128)(2,1)} %residual.1) | copy-start | bytes 1572868
  6.1 7.5 %copy-start.8 = (f32[2048]{0:T(1024)S(1)}, f32[2048]{0:T(1024)}, u32[]{:S(2)}) copy-start(f32[2048]{0:T(1024)} %param.20) | copy-start | bytes 24580
  6.3 5.4 %collective-permute-start.1 = (bf16[128,256]{1,0:T(8,128)(2,1)S(1)}, bf16[128,256]{1,0:T(8,128)(2,1)S(1)}, u32[]{:S(2)}, u32[]{:S(2)}) collective-permute-start(bf16[128,256]{1,0:T(8,128)(2,1)S(1)} %get-tuple-element.30), channel_id=1, source_target_pairs={{0,1},{1,2},{2,3},{3,0},{4,5},{5,6},{6,7},{7,4},{8,9},{9,10},{10,1... | collective-permute-start | bytes 196616 | tf_op jit(solution)/shard_map/ppermute | solution.py:257
  7.5 5.5 %collective-permute-start.2 = (bf16[128,256]{1,0:T(8,128)(2,1)S(1)}, bf16[128,256]{1,0:T(8,128)(2,1)S(1)}, u32[]{:S(2)}, u32[]{:S(2)}) collective-permute-start(bf16[128,256]{1,0:T(8,128)(2,1)S(1)} %get-tuple-element.31), channel_id=1, source_target_pairs={{0,2},{1,3},{2,0},{3,1},{4,6},{5,7},{6,4},{7,5},{8,10},{9,11},{10,... | collective-permute-start | bytes 196616 | tf_op jit(solution)/shard_map/ppermute | solution.py:257
  10.0 3.6 %collective-permute-start.3 = (bf16[128,256]{1,0:T(8,128)(2,1)S(1)}, bf16[128,256]{1,0:T(8,128)(2,1)S(1)}, u32[]{:S(2)}, u32[]{:S(2)}) collective-permute-start(bf16[128,256]{1,0:T(8,128)(2,1)S(1)} %get-tuple-element.32), channel_id=1, source_target_pairs={{0,3},{1,0},{2,1},{3,2},{4,7},{5,4},{6,5},{7,6},{8,11},{9,8},{10,9... | collective-permute-start | bytes 196616 | tf_op jit(solution)/shard_map/ppermute | solution.py:257
  13.6 44.2 %copy-start.2 = (bf16[1,2048,1024]{2,1,0:T(8,128)(2,1)S(1)}, bf16[1,2048,1024]{2,1,0:T(8,128)(2,1)}, u32[]{:S(2)}) copy-start(bf16[1,2048,1024]{2,1,0:T(8,128)(2,1)} %param.24) | copy-start | bytes 12582916
  13.6 44.2 %copy-start.3 = (bf16[1,1024,2048]{2,1,0:T(8,128)(2,1)S(1)}, bf16[1,1024,2048]{2,1,0:T(8,128)(2,1)}, u32[]{:S(2)}) copy-start(bf16[1,1024,2048]{2,1,0:T(8,128)(2,1)} %param.25) | copy-start | bytes 12582916
  15.3 42.5 %copy-start.1 = (bf16[1,2048,1024]{2,1,0:T(8,128)(2,1)S(1)}, bf16[1,2048,1024]{2,1,0:T(8,128)(2,1)}, u32[]{:S(2)}) copy-start(bf16[1,2048,1024]{2,1,0:T(8,128)(2,1)} %param.23) | copy-start | bytes 12582916
  64.5 34.2 %copy-start.12 = (f32[128,2]{0,1:T(2,128)S(1)}, f32[128,2]{0,1:T(2,128)}, u32[]{:S(2)}) copy-start(f32[128,2]{0,1:T(2,128)} %param.22) | copy-start | bytes 3076

commit v7 on v6

--- a/solution.py
+++ b/solution.py
@@ -14,7 +14,7 @@
 SLOT_FLOPS = 2 << 30
 EARLY_FLOPS = 8 << 30
 EDGE_FLOPS = 8 << 30
-ORDER = (2, 1, 3)
+ORDER = (1, 2, 3)
 VM = pl.BlockSpec(memory_space=pltpu.VMEM)
 SM = pl.BlockSpec(memory_space=pltpu.SMEM)
 HB = pl.BlockSpec(memory_space=pl.ANY)

time: 100 us -> 100 us (level)
  no operation moved by 1% of the time
where the time goes in v7:
time: 100 us
  blocking collectives  76.7 us (77%)
  Pallas kernels  11.8 us (12%)
  starting transfers between devices  9.47 us (9%)
  waiting for transfers between devices  2.03 us (2%)
    all_to_all x1, blocking collectives, on_device(): lax.all_to_all(buf.reshape(experts, 8, half), ('sp', 'tp'), split_axis=0,...  42.5 us
    all_to_all x1, blocking collectives, on_device(): lax.all_to_all(result.reshape(experts, 8, half), ('sp', 'tp'), split_axis...  34.2 us
    pallas_call x1, Pallas kernels, on_device(): call(expert_kernel, shape((rows, half), BF16), [VM] * 4, VM, [pltpu.VMEM(...  6.69 us
    ppermute x3, starting transfers between devices, on_device(): lax.ppermute(sent[d], 'tp', [(i, (i + d) % tp_count) for i in range(tp_co...  4.88 us
    ppermute x1, starting transfers between devices, on_device(): lax.ppermute(edge, 'sp', [(i, i + 1) for i in range(sp_count - 1)])  4.58 us
  transfers between devices with their start and end apart: 4, of which 3 were waited for; matrix products, arithmetic and copies ran while one was open for 0% of the time, Pallas kernels for 1%

profile of v7, /device:TPU:1, one launch (start us, length us, event | category | flops | bytes accessed | tf_op | source)
XLA Modules:
  0.0 100.2 jit_solution(6210852123552491948)
XLA Ops:
  0.0 0.0 copy-start.9
  0.0 0.0 copy-start.10
  0.0 0.8 edge.1
  0.9 4.6 %collective-permute-start = (f32[4,256]{1,0:T(4,128)S(1)}, f32[4,256]{1,0:T(4,128)S(1)}, u32[]{:S(2)}, u32[]{:S(2)}) collective-permute-start(f32[4,256]{1,0:T(4,128)S(1)} %edge.1), channel_id=1, source_target_pairs={{0,4},{4,8},{8,12},{12,16},{16,20},{20,24},{24,28},{28,32},{32,36}... | collective-permute-start | bytes 12296 | tf_op jit(solution)/shard_map/ppermute | solution.py:237
  5.4 0.0 copy-done.5
  5.5 0.0 copy-done.6
  5.5 0.0 copy-done.7
  5.5 0.0 copy-done.9
  5.5 0.0 copy-done.10
  5.5 0.0 copy-start.11
  5.5 0.5 early.1
  6.0 0.0 copy-start
  6.0 0.0 copy-start.4
  6.1 0.0 copy-start.8
  6.1 0.1 collective-permute-done.earlier
  6.2 0.1 fix.1
  6.3 1.3 %collective-permute-start.1 = (bf16[128,256]{1,0:T(8,128)(2,1)S(1)}, bf16[128,256]{1,0:T(8,128)(2,1)S(1)}, u32[]{:S(2)}, u32[]{:S(2)}) collective-permute-start(bf16[128,256]{1,0:T(8,128)(2,1)S(1)} %get-tuple-element.30), channel_id=1, source_target_pairs={{0,1},{1,2},{2,3},{3,0},{4,5},{5,6},{6,7},{7,4},{8,9},{9,10},{10,1... | collective-permute-start | bytes 196616 | tf_op jit(solution)/shard_map/ppermute | solution.py:257
  7.5 2.5 %collective-permute-start.2 = (bf16[128,256]{1,0:T(8,128)(2,1)S(1)}, bf16[128,256]{1,0:T(8,128)(2,1)S(1)}, u32[]{:S(2)}, u32[]{:S(2)}) collective-permute-start(bf16[128,256]{1,0:T(8,128)(2,1)S(1)} %get-tuple-element.31), channel_id=1, source_target_pairs={{0,2},{1,3},{2,0},{3,1},{4,6},{5,7},{6,4},{7,5},{8,10},{9,11},{10,... | collective-permute-start | bytes 196616 | tf_op jit(solution)/shard_map/ppermute | solution.py:257
  10.0 1.2 %collective-permute-start.3 = (bf16[128,256]{1,0:T(8,128)(2,1)S(1)}, bf16[128,256]{1,0:T(8,128)(2,1)S(1)}, u32[]{:S(2)}, u32[]{:S(2)}) collective-permute-start(bf16[128,256]{1,0:T(8,128)(2,1)S(1)} %get-tuple-element.32), channel_id=1, source_target_pairs={{0,3},{1,0},{2,1},{3,2},{4,7},{5,4},{6,5},{7,6},{8,11},{9,8},{10,9... | collective-permute-start | bytes 196616 | tf_op jit(solution)/shard_map/ppermute | solution.py:257
  11.2 0.5 slots.1
  11.7 0.0 collective-permute-done.1.r1
  11.7 1.4 %collective-permute-done.2.r2 = bf16[128,256]{1,0:T(8,128)(2,1)S(1)} collective-permute-done((bf16[128,256]{1,0:T(8,128)(2,1)S(1)}, bf16[128,256]{1,0:T(8,128)(2,1)S(1)}, u32[]{:S(2)}, u32[]{:S(2)}) %collective-permute-start.2) | collective-permute-done | bytes 65568 | tf_op jit(solution)/shard_map/ppermute | solution.py:257
  13.0 0.6 collective-permute-done.3.r3
  13.6 0.0 copy-start.2
  13.6 0.0 copy-start.3
  13.6 1.6 %mix.1 = (bf16[1024,1024]{1,0:T(8,128)(2,1)S(1)}, f32[128,2048]{1,0:T(8,128)S(1)}) custom-call(s32[1]{0:T(128)} %bitcast.place, bf16[128,256]{1,0:T(8,128)(2,1)S(1)} %get-tuple-element.29.r0, bf16[128,256]{1,0:T(8,128)(2,1)S(1)} %collective-permute-done.1.r1, bf16[128,256]{1,0:T(8,128)(2,1)S(1)} %collective-permute-done.2.r2, ...), custom_call_target="tpu_custom_call" | custom-call | flops 8589934592 | bytes 8388608 | tf_op jit(solution)/shard_map/mix/pallas_call | solution.py:262
  15.3 0.0 copy-start.1
  15.3 42.5 %all_to_all.10 = bf16[128,8,1024]{2,1,0:T(8,128)(2,1)S(1)} all-to-all(bf16[128,8,1024]{2,1,0:T(8,128)(2,1)S(1)} %bitcast.12), channel_id=1, replica_groups=mesh['sp'=32,'tp'=4] {'sp','tp'}, dimensions={0} | all-to-all | bytes 4194304 | tf_op jit(solution)/shard_map/all_to_all | solution.py:268
  57.8 6.7 %experts.1 = bf16[1024,1024]{1,0:T(8,128)(2,1)S(1)} custom-call(bf16[1024,1024]{1,0:T(8,128)(2,1)S(1)} %bitcast.14, bf16[2048,1024]{1,0:T(8,128)(2,1)S(1)} %bitcast.16, bf16[2048,1024]{1,0:T(8,128)(2,1)S(1)} %bitcast.17, bf16[1024,2048]{1,0:T(8,128)(2,1)S(1)} %bitcast.18), custom_call_target="tpu_custom_call" | custom-call | flops 6442450944 | bytes 16777216 | tf_op jit(solution)/shard_map/experts/pallas_call | solution.py:270
  64.5 0.0 copy-start.12
  64.5 34.2 %all_to_all.11 = bf16[128,8,1024]{2,1,0:T(8,128)(2,1)S(1)} all-to-all(bf16[128,8,1024]{2,1,0:T(8,128)(2,1)S(1)} %bitcast.15), channel_id=1, replica_groups=mesh['sp'=32,'tp'=4] {'sp','tp'}, dimensions={0} | all-to-all | bytes 4194304 | tf_op jit(solution)/shard_map/all_to_all | solution.py:278
  98.7 1.6 %combine.1 = bf16[128,2048]{1,0:T(8,128)(2,1)} custom-call(bf16[1024,1024]{1,0:T(8,128)(2,1)S(1)} %bitcast.13, f32[128,2048]{1,0:T(8,128)S(1)} %get-tuple-element.35.carried, bf16[256,512]{1,0:T(8,128)(2,1)S(1)} %get-tuple-element.36.pick, f32[2,128]{1,0:T(2,128)S(1)} %bitcast.23), custom_call_target="tpu_custom_call" | custom-call | flops 1073741824 | bytes 4194304 | tf_op jit(solution)/shard_map/combine/pallas_call | solution.py:279
  (11 shorter events, 0.0 us)
Async XLA Ops:
  0.0 5.4 %copy-start.5 = (bf16[512,256]{1,0:T(8,128)(2,1)S(1)}, bf16[512,256]{1,0:T(8,128)(2,1)}, u32[]{:S(2)}) copy-start(bf16[512,256]{1,0:T(8,128)(2,1)} %xv.1) | copy-start | bytes 786436
  0.0 5.5 %copy-start.6 = (bf16[512,256]{1,0:T(8,128)(2,1)S(1)}, bf16[512,256]{1,0:T(8,128)(2,1)}, u32[]{:S(2)}) copy-start(bf16[512,256]{1,0:T(8,128)(2,1)} %gv.1) | copy-start | bytes 786436
  0.0 5.5 %copy-start.7 = (bf16[512,256]{1,0:T(8,128)(2,1)S(1)}, bf16[512,256]{1,0:T(8,128)(2,1)}, u32[]{:S(2)}) copy-start(bf16[512,256]{1,0:T(8,128)(2,1)} %ov.1) | copy-start | bytes 786436
  0.0 5.5 %copy-start.9 = (s32[512]{0:T(512)S(1)}, s32[512]{0:T(512)}, u32[]{:S(2)}) copy-start(s32[512]{0:T(512)} %param.17) | copy-start | bytes 6148
  0.0 5.5 %copy-start.10 = (bf16[3,256]{1,0:T(4,128)(2,1)S(1)}, bf16[3,256]{1,0:T(4,128)(2,1)}, u32[]{:S(2)}) copy-start(bf16[3,256]{1,0:T(4,128)(2,1)} %taps.1) | copy-start | bytes 4612
  0.9 5.3 %collective-permute-start = (f32[4,256]{1,0:T(4,128)S(1)}, f32[4,256]{1,0:T(4,128)S(1)}, u32[]{:S(2)}, u32[]{:S(2)}) collective-permute-start(f32[4,256]{1,0:T(4,128)S(1)} %edge.1), channel_id=1, source_target_pairs={{0,4},{4,8},{8,12},{12,16},{16,20},{20,24},{24,28},{28,32},{32,36}... | collective-permute-start | bytes 12296 | tf_op jit(solution)/shard_map/ppermute | solution.py:237
  5.5 5.7 %copy-start.11 = (s32[128,2]{0,1:T(2,128)S(1)}, s32[128,2]{0,1:T(2,128)}, u32[]{:S(2)}) copy-start(s32[128,2]{0,1:T(2,128)} %param.21) | copy-start | bytes 3076
  6.0 7.6 %copy-start = (bf16[1024,2048]{1,0:T(8,128)(2,1)S(1)}, bf16[1024,2048]{1,0:T(8,128)(2,1)}, u32[]{:S(2)}) copy-start(bf16[1024,2048]{1,0:T(8,128)(2,1)} %proj.1) | copy-start | bytes 12582916
  6.0 7.5 %copy-start.4 = (bf16[128,2048]{1,0:T(8,128)(2,1)S(1)}, bf16[128,2048]{1,0:T(8,128)(2,1)}, u32[]{:S(2)}) copy-start(bf16[128,2048]{1,0:T(8,128)(2,1)} %residual.1) | copy-start | bytes 1572868
  6.1 7.5 %copy-start.8 = (f32[2048]{0:T(1024)S(1)}, f32[2048]{0:T(1024)}, u32[]{:S(2)}) copy-start(f32[2048]{0:T(1024)} %param.20) | copy-start | bytes 24580
  6.3 5.4 %collective-permute-start.1 = (bf16[128,256]{1,0:T(8,128)(2,1)S(1)}, bf16[128,256]{1,0:T(8,128)(2,1)S(1)}, u32[]{:S(2)}, u32[]{:S(2)}) collective-permute-start(bf16[128,256]{1,0:T(8,128)(2,1)S(1)} %get-tuple-element.30), channel_id=1, source_target_pairs={{0,1},{1,2},{2,3},{3,0},{4,5},{5,6},{6,7},{7,4},{8,9},{9,10},{10,1... | collective-permute-start | bytes 196616 | tf_op jit(solution)/shard_map/ppermute | solution.py:257
  7.5 5.5 %collective-permute-start.2 = (bf16[128,256]{1,0:T(8,128)(2,1)S(1)}, bf16[128,256]{1,0:T(8,128)(2,1)S(1)}, u32[]{:S(2)}, u32[]{:S(2)}) collective-permute-start(bf16[128,256]{1,0:T(8,128)(2,1)S(1)} %get-tuple-element.31), channel_id=1, source_target_pairs={{0,2},{1,3},{2,0},{3,1},{4,6},{5,7},{6,4},{7,5},{8,10},{9,11},{10,... | collective-permute-start | bytes 196616 | tf_op jit(solution)/shard_map/ppermute | solution.py:257
  10.0 3.6 %collective-permute-start.3 = (bf16[128,256]{1,0:T(8,128)(2,1)S(1)}, bf16[128,256]{1,0:T(8,128)(2,1)S(1)}, u32[]{:S(2)}, u32[]{:S(2)}) collective-permute-start(bf16[128,256]{1,0:T(8,128)(2,1)S(1)} %get-tuple-element.32), channel_id=1, source_target_pairs={{0,3},{1,0},{2,1},{3,2},{4,7},{5,4},{6,5},{7,6},{8,11},{9,8},{10,9... | collective-permute-start | bytes 196616 | tf_op jit(solution)/shard_map/ppermute | solution.py:257
  13.6 44.2 %copy-start.2 = (bf16[1,2048,1024]{2,1,0:T(8,128)(2,1)S(1)}, bf16[1,2048,1024]{2,1,0:T(8,128)(2,1)}, u32[]{:S(2)}) copy-start(bf16[1,2048,1024]{2,1,0:T(8,128)(2,1)} %param.24) | copy-start | bytes 12582916
  13.6 44.2 %copy-start.3 = (bf16[1,1024,2048]{2,1,0:T(8,128)(2,1)S(1)}, bf16[1,1024,2048]{2,1,0:T(8,128)(2,1)}, u32[]{:S(2)}) copy-start(bf16[1,1024,2048]{2,1,0:T(8,128)(2,1)} %param.25) | copy-start | bytes 12582916
  15.3 42.5 %copy-start.1 = (bf16[1,2048,1024]{2,1,0:T(8,128)(2,1)S(1)}, bf16[1,2048,1024]{2,1,0:T(8,128)(2,1)}, u32[]{:S(2)}) copy-start(bf16[1,2048,1024]{2,1,0:T(8,128)(2,1)} %param.23) | copy-start | bytes 12582916
  64.5 34.2 %copy-start.12 = (f32[128,2]{0,1:T(2,128)S(1)}, f32[128,2]{0,1:T(2,128)}, u32[]{:S(2)}) copy-start(f32[128,2]{0,1:T(2,128)} %param.22) | copy-start | bytes 3076
